TPU v7x, 32 devices: a whole 2x2x4 slice. The times are simulated.
32 devices in a mesh: sp: 16 (over z, y, x), tp: 2 (over core).
Axes of the slice: x: 2, y: 2, z: 4, core: 2. Of those that a mesh axis runs over, the one named last changes fastest.
Arguments:
- residual_in: bfloat16 [4096, 2048], P('sp'), may hold values from -6 to 6
- mixer_input: bfloat16 [2048, 4096], P('tp', 'sp'), may hold values from -6 to 6
- branch_gate: bfloat16 [2048, 4096], P('tp', 'sp'), may hold values from -6 to 6
- conv_taps: bfloat16 [2048, 4], P('tp'), may hold values from -3 to 3
- recur_weight: bfloat16 [32, 64, 64], P('tp'), may hold values from -0.75 to 0.75
- admit_weight: bfloat16 [32, 64, 64], P('tp'), may hold values from -0.75 to 0.75
- decay_param: float32 [2048], P('tp'), may hold values from 4 to 16
- decay_extra: float32 [2048, 4096], P('tp', 'sp'), may hold values from -1 to 0
- out_weight: bfloat16 [2048, 2048], P('tp'), may hold values from -0.375 to 0.375
- norm_gain: bfloat16 [2048], replicated, may hold values from 0.099609375 to 1.8984375
- gate_weight: bfloat16 [2048, 5632], P('sp', 'tp'), may hold values from -0.125 to 0.125
- up_weight: bfloat16 [2048, 5632], P('sp', 'tp'), may hold values from -0.125 to 0.125
- down_weight: bfloat16 [2048, 5632], P('sp', 'tp'), may hold values from -0.15625 to 0.15625
Outputs:
- layer_out: bfloat16 [4096, 2048], P('sp')
All inputs are finite; a program needn't handle non-finite values.
Results may differ from a plain program's by a relative error of at most 0.019.
Values may be sent and summed in bfloat16 or wider, within the bound.
A program may use at most 128 MiB of HBM per device.

v0:
```python
import functools

import jax
import jax.numpy as jnp
from jax import lax
from jax.experimental import pallas as pl
from jax.experimental.pallas import tpu as pltpu
from jax.sharding import PartitionSpec as P

MESH = pl.DeviceIdType.MESH
LANES = 128


def neg_expm1(v):
    series = jnp.full_like(v, 1.0)
    for k in range(9, 1, -1):
        series = 1.0 + series * v * (1.0 / k)
    return jnp.where(v > -0.5, -v * series, 1.0 - jnp.exp(v))


def mixer_kernel(
    n,
    x_ref,
    halo_ref,
    bg_ref,
    extra_ref,
    taps_ref,
    rate_ref,
    wr_ref,
    wa_ref,
    out_ref,
    state_s,
    run_s,
    ends_s,
    all_s,
    in_s,
    send_sem,
    recv_sem,
):
    me = lax.axis_index("sp")
    barrier = pltpu.get_barrier_semaphore()

    def greet(k, carry):
        pl.semaphore_signal(
            barrier, inc=1, device_id={"sp": lax.rem(me + k, n)}, device_id_type=MESH
        )
        return carry

    lax.fori_loop(1, n, greet, 0)
    channels, length = x_ref.shape
    block = wr_ref.shape[1]
    groups = channels // LANES
    tap_count = taps_ref.shape[1]
    lane = lax.broadcasted_iota(jnp.int32, (LANES, length), 1)

    def local(g, carry):
        rows = pl.ds(pl.multiple_of(g * LANES, LANES), LANES)
        wide = jnp.concatenate(
            [halo_ref[rows, :].astype(jnp.float32), x_ref[rows, :].astype(jnp.float32)], axis=1
        )
        taps = taps_ref[rows, :]
        total = taps[:, tap_count - 1 :] * wide[:, LANES:]
        for tap in range(tap_count - 2, -1, -1):
            total = total + taps[:, tap : tap + 1] * pltpu.roll(wide, tap_count - 1 - tap, 1)[:, LANES:]
        conv = total.astype(jnp.bfloat16)
        per = LANES // block
        recur, admit = [], []
        for b in range(per):
            part = conv[b * block : (b + 1) * block]
            recur.append(jnp.dot(wr_ref[g * per + b], part, preferred_element_type=jnp.float32))
            admit.append(jnp.dot(wa_ref[g * per + b], part, preferred_element_type=jnp.float32))
        recur = jax.nn.sigmoid(jnp.concatenate(recur, axis=0))
        admit = jax.nn.sigmoid(jnp.concatenate(admit, axis=0))
        log_decay = recur * rate_ref[rows, :] + extra_ref[rows, :]
        a = jnp.exp(log_decay)
        b = jnp.sqrt(neg_expm1(2.0 * log_decay)) * admit * conv.astype(jnp.float32)
        shift = 1
        while shift < length:
            seen = lane >= shift
            b = b + a * jnp.where(seen, pltpu.roll(b, shift, 1), 0.0)
            a = a * jnp.where(seen, pltpu.roll(a, shift, 1), 1.0)
            shift *= 2
        state_s[rows, :] = b
        run_s[rows, :] = a
        ends_s[pl.ds(g, 1), :] = a[:, length - LANES :].T[LANES - 1 :]
        ends_s[pl.ds(groups + g, 1), :] = b[:, length - LANES :].T[LANES - 1 :]
        return carry

    lax.fori_loop(0, groups, local, 0)
    pl.semaphore_wait(barrier, n - 1)

    def copy_to(k):
        return pltpu.make_async_remote_copy(
            src_ref=ends_s,
            dst_ref=all_s.at[k - 1],
            send_sem=send_sem.at[k - 1],
            recv_sem=recv_sem.at[k - 1],
            device_id={"sp": lax.rem(me + k, n)},
            device_id_type=MESH,
        )

    def send(k, carry):
        copy_to(k).start()
        return carry

    lax.fori_loop(1, n, send, 0)

    def finish(k, carry):
        copy_to(k).wait()
        return carry

    lax.fori_loop(1, n, finish, 0)

    def fold(i, before):
        k = n - 1 - i
        part = all_s[k - 1]
        new = part[:groups] * before + part[groups:]
        return jnp.where(k <= me, new, before)

    in_s[...] = lax.fori_loop(0, n - 1, fold, jnp.zeros((groups, LANES), jnp.float32))

    def close(g, carry):
        rows = pl.ds(pl.multiple_of(g * LANES, LANES), LANES)
        entering = jnp.broadcast_to(in_s[pl.ds(g, 1), :], (LANES, LANES)).T
        entering = jnp.concatenate([entering] * (length // LANES), axis=1)
        states = state_s[rows, :] + run_s[rows, :] * entering
        v = bg_ref[rows, :].astype(jnp.float32)
        act = 0.5 * v * (1.0 + jnp.tanh(0.7978845608028654 * (v + 0.044715 * v * v * v)))
        out_ref[rows, :] = (states * act).astype(jnp.bfloat16)
        return carry

    lax.fori_loop(0, groups, close, 0)


def mixer(n, x, halo, bg, extra, taps, rate, wr, wa):
    channels, length = x.shape
    groups = channels // LANES
    vmem = pl.BlockSpec(memory_space=pltpu.VMEM)
    return pl.pallas_call(
        functools.partial(mixer_kernel, n),
        out_shape=jax.ShapeDtypeStruct((channels, length), jnp.bfloat16),
        in_specs=[vmem] * 8,
        out_specs=vmem,
        scratch_shapes=[
            pltpu.VMEM((channels, length), jnp.float32),
            pltpu.VMEM((channels, length), jnp.float32),
            pltpu.VMEM((2 * groups, LANES), jnp.float32),
            pltpu.VMEM((n - 1, 2 * groups, LANES), jnp.float32),
            pltpu.VMEM((groups, LANES), jnp.float32),
            pltpu.SemaphoreType.DMA((n - 1,)),
            pltpu.SemaphoreType.DMA((n - 1,)),
        ],
        compiler_params=pltpu.CompilerParams(
            collective_id=0, has_side_effects=True, vmem_limit_bytes=24 << 20
        ),
        cost_estimate=pl.CostEstimate(
            flops=200 * channels * length, bytes_accessed=12 * channels * length, transcendentals=0
        ),
        name="mixer",
    )(x, halo, bg, extra, taps, rate, wr, wa)


def layer_kernel(
    n,
    split,
    x_ref,
    bg_ref,
    extra_ref,
    taps_ref,
    rate_ref,
    wr_ref,
    wa_ref,
    ow_ref,
    res_ref,
    gain_ref,
    packed_ref,
    wide_ref,
    tok_ref,
    mid_ref,
    halo_ref,
    state_s,
    run_s,
    ends_s,
    all_s,
    in_s,
    mix_s,
    part_s,
    part_r,
    nrm_s,
    own_s,
    send_sem,
    recv_sem,
    zs_sem,
    zr_sem,
    ps_sem,
    pr_sem,
    fs_sem,
    fr_sem,
    ts_sem,
    tr_sem,
    bs_sem,
    br_sem,
    cs_sem,
    cr_sem,
    own_sem,
    hs_sem,
    hr_sem,
    rs_sem,
    rr_sem,
):
    me = lax.axis_index("sp")
    core = lax.axis_index("tp")
    plane = n // split
    rank, spot = me // plane, lax.rem(me, plane)
    barrier = pltpu.get_barrier_semaphore()

    def greet(k, carry):
        pl.semaphore_signal(
            barrier, inc=1, device_id={"sp": lax.rem(me + k, n)}, device_id_type=MESH
        )
        return carry

    lax.fori_loop(1, n, greet, 0)
    pl.semaphore_signal(barrier, inc=1, device_id={"tp": 1 - core}, device_id_type=MESH)
    pl.semaphore_wait(barrier, n)

    depth = packed_ref.shape[3]
    span = packed_ref.shape[2]
    kinds = packed_ref.shape[1]

    def columns(source):
        return pl.ds(pl.multiple_of(source * depth, depth), depth)

    def remote(src, dst, ssem, rsem, where):
        return pltpu.make_async_remote_copy(
            src_ref=src, dst_ref=dst, send_sem=ssem, recv_sem=rsem,
            device_id=where, device_id_type=MESH,
        )

    def z_copy(c, k):
        to = lax.rem(rank + k, split)
        return remote(
            packed_ref.at[to, c], wide_ref.at[c, :, columns(me)],
            zs_sem.at[c, k - 1], zr_sem.at[c, k - 1], {"sp": to * plane + spot},
        )

    def z_landed(c, k):
        source = lax.rem(rank - k + split, split) * plane + spot
        return remote(
            packed_ref.at[rank, c], wide_ref.at[c, :, columns(source)],
            zs_sem.at[c, k - 1], zr_sem.at[c, k - 1], {"sp": source},
        )

    def beside(m):
        return spot + 1 - 2 * lax.rem(spot, 2) if m == 1 else spot + 2 - 4 * (spot // 2)

    def own_copy(c, m):
        return remote(
            packed_ref.at[rank, c], wide_ref.at[c, :, columns(me)],
            ps_sem.at[c, m - 1], pr_sem.at[c, m - 1],
            {"sp": rank * plane + beside(m)},
        )

    def own_landed(c, m):
        source = rank * plane + beside(m)
        return remote(
            packed_ref.at[rank, c], wide_ref.at[c, :, columns(source)],
            ps_sem.at[c, m - 1], pr_sem.at[c, m - 1], {"sp": source},
        )

    def pass_copy(c, k, m):
        source = lax.rem(rank - k + split, split) * plane + spot
        window = wide_ref.at[c, :, columns(source)]
        return remote(
            window, window, fs_sem.at[c, k - 1, m - 1], fr_sem.at[c, k - 1, m - 1],
            {"sp": rank * plane + beside(m)},
        )

    def pass_landed(c, k, m):
        behind = beside(m)
        source = lax.rem(rank - k + split, split) * plane + behind
        window = wide_ref.at[c, :, columns(source)]
        return remote(
            window, window, fs_sem.at[c, k - 1, m - 1], fr_sem.at[c, k - 1, m - 1],
            {"sp": rank * plane + behind},
        )

    def relay_window(c, k, m, where):
        source = lax.rem(rank - k + split, split) * plane + where
        return wide_ref.at[c, pl.ds((m - 1) * (span // 2), span // 2), columns(source)]

    def relay_copy(c, k, m):
        window = relay_window(c, k, m, beside(m))
        return remote(
            window, window, rs_sem.at[c, k, m - 1], rr_sem.at[c, k, m - 1],
            {"sp": rank * plane + beside(3 - m)},
        )

    def relay_landed(c, k, m):
        window = relay_window(c, k, m, 3 - spot)
        return remote(
            window, window, rs_sem.at[c, k, m - 1], rr_sem.at[c, k, m - 1],
            {"sp": rank * plane + beside(3 - m)},
        )

    def relay(c, k):
        for m in (1, 2):
            landed = pass_landed(c, k, m) if k else own_landed(c, m)
            landed.wait_recv()
            relay_copy(c, k, m).start()

    def z_start(c):
        for k in range(1, split):
            z_copy(c, k).start()

    def z_pass(c):
        for k in range(1, split):
            z_landed(c, k).wait_recv()
            for m in (1, 2):
                pass_copy(c, k, m).start()

    halo_copy = remote(
        x_ref.at[:, pl.ds(x_ref.shape[1] - LANES, LANES)], halo_ref, hs_sem, hr_sem,
        {"sp": lax.rem(me + 1, n)},
    )
    halo_copy.start()
    z_start(0)
    for c in range(kinds):
        for m in (1, 2):
            own_copy(c, m).start()
    own_in = pltpu.make_async_copy(packed_ref.at[rank], own_s, own_sem.at[0])
    own_in.start()
    halo_copy.wait()
    inside = jnp.where(me > 0, 1.0, 0.0)
    channels, length = x_ref.shape
    block = wr_ref.shape[1]
    groups = channels // LANES
    tap_count = taps_ref.shape[1]
    lane = lax.broadcasted_iota(jnp.int32, (LANES, length), 1)

    def local(g, carry):
        rows = pl.ds(pl.multiple_of(g * LANES, LANES), LANES)
        wide = jnp.concatenate(
            [halo_ref[rows, :].astype(jnp.float32) * inside, x_ref[rows, :].astype(jnp.float32)], axis=1
        )
        taps = taps_ref[rows, :]
        total = taps[:, tap_count - 1 :] * wide[:, LANES:]
        for tap in range(tap_count - 2, -1, -1):
            total = total + taps[:, tap : tap + 1] * pltpu.roll(wide, tap_count - 1 - tap, 1)[:, LANES:]
        conv = total.astype(jnp.bfloat16)
        per = LANES // block
        recur, admit = [], []
        for b in range(per):
            part = conv[b * block : (b + 1) * block]
            recur.append(jnp.dot(wr_ref[g * per + b], part, preferred_element_type=jnp.float32))
            admit.append(jnp.dot(wa_ref[g * per + b], part, preferred_element_type=jnp.float32))
        recur = jax.nn.sigmoid(jnp.concatenate(recur, axis=0))
        admit = jax.nn.sigmoid(jnp.concatenate(admit, axis=0))
        log_decay = recur * rate_ref[rows, :] + extra_ref[rows, :]
        a = jnp.exp(log_decay)
        b = jnp.sqrt(neg_expm1(2.0 * log_decay)) * admit * conv.astype(jnp.float32)
        shift = 1
        while shift < length:
            seen = lane >= shift
            b = b + a * jnp.where(seen, pltpu.roll(b, shift, 1), 0.0)
            a = a * jnp.where(seen, pltpu.roll(a, shift, 1), 1.0)
            shift *= 2
        state_s[rows, :] = b
        run_s[rows, :] = a
        ends_s[pl.ds(g, 1), :] = a[:, length - LANES :].T[LANES - 1 :]
        ends_s[pl.ds(groups + g, 1), :] = b[:, length - LANES :].T[LANES - 1 :]
        return carry

    lax.fori_loop(0, groups, local, 0)

    own_in.wait()
    own_out = pltpu.make_async_copy(own_s, wide_ref.at[:, :, columns(me)], own_sem.at[1])
    own_out.start()
    relay(0, 0)
    z_pass(0)
    z_start(1)
    def copy_to(k):
        return pltpu.make_async_remote_copy(
            src_ref=ends_s,
            dst_ref=all_s.at[k - 1],
            send_sem=send_sem.at[k - 1],
            recv_sem=recv_sem.at[k - 1],
            device_id={"sp": lax.rem(me + k, n)},
            device_id_type=MESH,
        )

    def send(k, carry):
        copy_to(k).start()
        return carry

    lax.fori_loop(1, n, send, 0)

    def finish(k, carry):
        copy_to(k).wait()
        return carry

    lax.fori_loop(1, n, finish, 0)

    def fold(i, before):
        k = n - 1 - i
        part = all_s[k - 1]
        new = part[:groups] * before + part[groups:]
        return jnp.where(k <= me, new, before)

    in_s[...] = lax.fori_loop(0, n - 1, fold, jnp.zeros((groups, LANES), jnp.float32))

    def close(g, carry):
        rows = pl.ds(pl.multiple_of(g * LANES, LANES), LANES)
        entering = jnp.broadcast_to(in_s[pl.ds(g, 1), :], (LANES, LANES)).T
        entering = jnp.concatenate([entering] * (length // LANES), axis=1)
        states = state_s[rows, :] + run_s[rows, :] * entering
        v = bg_ref[rows, :].astype(jnp.float32)
        act = 0.5 * v * (1.0 + jnp.tanh(0.7978845608028654 * (v + 0.044715 * v * v * v)))
        mix_s[:, rows] = (states * act).T.astype(jnp.bfloat16)
        return carry

    lax.fori_loop(0, groups, close, 0)

    pieces, row_count, cut = part_s.shape

    def swap(i):
        return remote(
            part_s.at[i], part_r.at[i], bs_sem.at[i], br_sem.at[i], {"tp": 1 - core}
        )

    for i in range(pieces):
        part_s[i] = jnp.dot(
            mix_s[...], ow_ref[:, i * cut : (i + 1) * cut], preferred_element_type=jnp.float32
        ).astype(jnp.bfloat16)
        if i:
            swap(i - 1).start()
    z_pass(1)
    z_start(2)
    swap(pieces - 1).start()
    square = jnp.zeros((row_count, 1), jnp.float32)
    for i in range(pieces):
        swap(i).wait()
        cols = slice(i * cut, (i + 1) * cut)
        branch = part_s[i].astype(jnp.float32) + part_r[i].astype(jnp.float32)
        middle = (res_ref[:, cols].astype(jnp.float32) + branch).astype(jnp.bfloat16)
        mid_ref[:, cols] = middle
        middle = middle.astype(jnp.float32)
        square = square + jnp.sum(middle * middle, axis=1, keepdims=True)
    scale = lax.rsqrt(square * (1.0 / (pieces * cut)) + 1e-06)
    for i in range(pieces):
        cols = slice(i * cut, (i + 1) * cut)
        middle = mid_ref[:, cols].astype(jnp.float32)
        nrm_s[:, cols] = (middle * scale * gain_ref[:, cols].astype(jnp.float32)).astype(jnp.bfloat16)
    half = row_count // 2
    mine = pl.ds(pl.multiple_of(core * half, half), half)
    other = pl.ds(pl.multiple_of((1 - core) * half, half), half)

    def tok_copy(k):
        to = lax.rem(rank + k, split)
        return remote(
            nrm_s.at[mine, :], tok_ref.at[rank, mine, :],
            ts_sem.at[k - 1], tr_sem.at[k - 1], {"sp": to * plane + spot},
        )

    def tok_landed(k):
        source = lax.rem(rank - k + split, split)
        return remote(
            nrm_s.at[mine, :], tok_ref.at[source, mine, :],
            ts_sem.at[k - 1], tr_sem.at[k - 1], {"sp": source * plane + spot},
        )

    def tok_pass(k, rows):
        source = lax.rem(rank - k + split, split)
        window = tok_ref.at[source, rows, :]
        return remote(window, window, cs_sem.at[k - 1], cr_sem.at[k - 1], {"tp": 1 - core})

    for k in range(1, split):
        tok_copy(k).start()
    own_tok = pltpu.make_async_copy(nrm_s, tok_ref.at[rank], own_sem.at[2])
    own_tok.start()
    relay(1, 0)
    relay(2, 0)
    for k in range(1, split):
        relay(0, k)
    z_pass(2)
    for k in range(1, split):
        relay(1, k)
    for k in range(1, split):
        tok_landed(k).wait_recv()
        tok_pass(k, mine).start()
    for k in range(1, split):
        tok_copy(k).wait_send()
        tok_pass(k, mine).wait_send()
        tok_pass(k, other).wait_recv()
    own_tok.wait()
    own_out.wait()
    for k in range(1, split):
        relay(2, k)
    for c in range(kinds):
        for m in (1, 2):
            own_copy(c, m).wait_send()
        for k in range(split):
            for m in (1, 2):
                if k:
                    pass_copy(c, k, m).wait_send()
                relay_copy(c, k, m).wait_send()
                relay_landed(c, k, m).wait_recv()
            if k:
                z_copy(c, k).wait_send()


def layer_front(n, split, x, bg, extra, taps, rate, wr, wa, ow, res, gain, packed):
    channels, length = x.shape
    groups = channels // LANES
    rows, width = res.shape
    kinds, span, depth = packed.shape[1:]
    plane = n // split
    cut = 512
    pieces = width // cut
    vmem = pl.BlockSpec(memory_space=pltpu.VMEM)
    hbm = pl.BlockSpec(memory_space=pl.ANY)
    dma = pltpu.SemaphoreType.DMA
    bf16, f32 = jnp.bfloat16, jnp.float32
    return pl.pallas_call(
        functools.partial(layer_kernel, n, split),
        out_shape=(
            jax.ShapeDtypeStruct((kinds, span, n * depth), bf16),
            jax.ShapeDtypeStruct((split, rows, width), bf16),
            jax.ShapeDtypeStruct((rows, width), bf16),
        ),
        in_specs=[vmem] * 10 + [hbm],
        out_specs=(hbm, hbm, vmem),
        scratch_shapes=[
            pltpu.VMEM((channels, LANES), bf16),
            pltpu.VMEM((channels, length), f32),
            pltpu.VMEM((channels, length), f32),
            pltpu.VMEM((2 * groups, LANES), f32),
            pltpu.VMEM((n - 1, 2 * groups, LANES), f32),
            pltpu.VMEM((groups, LANES), f32),
            pltpu.VMEM((length, channels), bf16),
            pltpu.VMEM((pieces, rows, cut), bf16),
            pltpu.VMEM((pieces, rows, cut), bf16),
            pltpu.VMEM((rows, width), bf16),
            pltpu.VMEM((kinds, span, depth), bf16),
            dma((n - 1,)),
            dma((n - 1,)),
            dma((kinds, split - 1)),
            dma((kinds, split - 1)),
            dma((kinds, 2)),
            dma((kinds, 2)),
            dma((kinds, split - 1, 2)),
            dma((kinds, split - 1, 2)),
            dma((split - 1,)),
            dma((split - 1,)),
            dma((pieces,)),
            dma((pieces,)),
            dma((split - 1,)),
            dma((split - 1,)),
            dma((3,)),
            dma,
            dma,
            dma((kinds, split, 2)),
            dma((kinds, split, 2)),
        ],
        compiler_params=pltpu.CompilerParams(
            collective_id=1, has_side_effects=True, vmem_limit_bytes=40 << 20
        ),
        name="layer_front",
    )(x, bg, extra, taps, rate, wr, wa, ow, res, gain, packed)


def close_kernel(
    n, split, tok_ref, wide_ref, mid_ref, out_ref,
    part_ref, tok_s, wide_s, tk_sem, wd_sem, tp_s, red_s, z_s, half_s, half_r,
    as_sem, ar_sem, zs_sem, zr_sem, hs_sem, hr_sem,
):
    me = lax.axis_index("sp")
    core = lax.axis_index("tp")
    plane = n // split
    rank, spot = me // plane, lax.rem(me, plane)
    barrier = pltpu.get_barrier_semaphore()
    order = list(range(1, split)) + [0]
    kinds = wide_ref.shape[0]

    def tok_in(k):
        return pltpu.make_async_copy(
            tok_ref.at[lax.rem(rank + k, split)], tok_s.at[k], tk_sem.at[k]
        )

    def wide_in(c):
        return pltpu.make_async_copy(wide_ref.at[c], wide_s.at[c], wd_sem.at[c])

    tok_in(order[0]).start()
    for c in range(kinds):
        wide_in(c).start()
    for k in order[1:]:
        tok_in(k).start()
    for k in range(1, split):
        pl.semaphore_signal(
            barrier, inc=1,
            device_id={"sp": lax.rem(rank + k, split) * plane + spot}, device_id_type=MESH,
        )
    pl.semaphore_signal(barrier, inc=1, device_id={"tp": 1 - core}, device_id_type=MESH)
    def feed(k):
        tok_in(k).wait()
        across = (((1,), (1,)), ((), ()))
        if k == order[0]:
            wide_in(0).wait()
        gate = lax.dot_general(tok_s[k], wide_s[0], across, preferred_element_type=jnp.float32)
        if k == order[0]:
            wide_in(1).wait()
        up = lax.dot_general(tok_s[k], wide_s[1], across, preferred_element_type=jnp.float32)
        hidden = (gate / (1.0 + jnp.exp(-gate)) * up).astype(jnp.bfloat16)
        if k == order[0]:
            wide_in(2).wait()
        part_ref[k] = jnp.dot(
            hidden, wide_s[2], preferred_element_type=jnp.float32
        ).astype(jnp.bfloat16)

    half = mid_ref.shape[0] // 2
    mine = pl.ds(pl.multiple_of(core * half, half), half)
    other = pl.ds(pl.multiple_of((1 - core) * half, half), half)

    def to_rank(k):
        return lax.rem(rank + k, split)

    def tp_copy(k):
        return pltpu.make_async_remote_copy(
            src_ref=part_ref.at[k, other, :], dst_ref=tp_s.at[k],
            send_sem=as_sem.at[k], recv_sem=ar_sem.at[k],
            device_id={"tp": 1 - core}, device_id_type=MESH,
        )

    def z_copy(k):
        return pltpu.make_async_remote_copy(
            src_ref=red_s.at[k - 1], dst_ref=z_s.at[k - 1],
            send_sem=zs_sem.at[k - 1], recv_sem=zr_sem.at[k - 1],
            device_id={"sp": to_rank(k) * plane + spot}, device_id_type=MESH,
        )

    def reduce(k):
        tp_copy(k).wait()
        mixed = part_ref[k, mine, :].astype(jnp.float32) + tp_s[k].astype(jnp.float32)
        red_s[k - 1] = mixed.astype(jnp.bfloat16)

    feed(1)
    pl.semaphore_wait(barrier, split)
    tp_copy(1).start()
    for k in range(2, split):
        feed(k)
        tp_copy(k).start()
        reduce(k - 1)
        z_copy(k - 1).start()
    reduce(split - 1)
    z_copy(split - 1).start()
    feed(0)
    tp_copy(0).start()
    tp_copy(0).wait()
    total = part_ref[0, mine, :].astype(jnp.float32) + tp_s[0].astype(jnp.float32)
    for k in range(1, split):
        z_copy(k).wait()
        total = total + z_s[k - 1].astype(jnp.float32)
    done = (mid_ref[mine, :].astype(jnp.float32) + total).astype(jnp.bfloat16)
    half_s[...] = done
    out_ref[mine, :] = done
    last = pltpu.make_async_remote_copy(
        src_ref=half_s, dst_ref=half_r, send_sem=hs_sem, recv_sem=hr_sem,
        device_id={"tp": 1 - core}, device_id_type=MESH,
    )
    last.start()
    last.wait()
    out_ref[other, :] = half_r[...]


def layer_close(n, split, tokens, wide, middle):
    rows, width = middle.shape
    half = rows // 2
    vmem = pl.BlockSpec(memory_space=pltpu.VMEM)
    dma = pltpu.SemaphoreType.DMA
    bf16 = jnp.bfloat16
    return pl.pallas_call(
        functools.partial(close_kernel, n, split),
        out_shape=jax.ShapeDtypeStruct((rows, width), bf16),
        in_specs=[pl.BlockSpec(memory_space=pl.ANY)] * 2 + [vmem],
        out_specs=vmem,
        scratch_shapes=[
            pltpu.VMEM((split, rows, width), bf16),
            pltpu.VMEM((split, rows, width), bf16),
            pltpu.VMEM(wide.shape, bf16),
            dma((split,)),
            dma((wide.shape[0],)),
            pltpu.VMEM((split, half, width), bf16),
            pltpu.VMEM((split - 1, half, width), bf16),
            pltpu.VMEM((split - 1, half, width), bf16),
            pltpu.VMEM((half, width), bf16),
            pltpu.VMEM((half, width), bf16),
            dma((split,)),
            dma((split,)),
            dma((split - 1,)),
            dma((split - 1,)),
            dma,
            dma,
        ],
        compiler_params=pltpu.CompilerParams(
            collective_id=2, has_side_effects=True, vmem_limit_bytes=48 << 20
        ),
        name="layer_close",
    )(tokens, wide, middle)


def on_device(
    residual_in,
    mixer_input,
    branch_gate,
    conv_taps,
    recur_weight,
    admit_weight,
    decay_param,
    decay_extra,
    out_weight,
    norm_gain,
    gate_weight,
    up_weight,
    down_weight,
):
    n = lax.axis_size("sp")
    length = mixer_input.shape[1]
    halo = lax.ppermute(
        mixer_input[:, length - LANES :], "sp", [(i, i + 1) for i in range(n - 1)]
    )
    rate = -8.0 * jax.nn.softplus(-decay_param)[:, None]
    width, share_ff = residual_in.shape[1], gate_weight.shape[1]
    split = 4
    if (
        lax.axis_size("tp") == 2
        and n == 4 * split
        and gate_weight.shape[0] % LANES == 0
        and share_ff % (32 * split) == 0
        and width % 512 == 0
    ):
        span = share_ff // split
        packed = jnp.stack(
            [
                w.reshape(w.shape[0], split, span).transpose(1, 2, 0)
                for w in (gate_weight, up_weight, down_weight)
            ],
            axis=1,
        )
        wide, tokens, middle = layer_front(
            n,
            split,
            mixer_input,
            branch_gate,
            decay_extra,
            conv_taps.astype(jnp.float32),
            rate,
            recur_weight.transpose(0, 2, 1),
            admit_weight.transpose(0, 2, 1),
            out_weight,
            residual_in,
            norm_gain.reshape(1, width),
            packed,
        )
        return layer_close(n, split, tokens, wide, middle)
    mixed_out = mixer(
        n,
        mixer_input,
        halo,
        branch_gate,
        decay_extra,
        conv_taps.astype(jnp.float32),
        rate,
        recur_weight.transpose(0, 2, 1),
        admit_weight.transpose(0, 2, 1),
    )
    row_count = residual_in.shape[0]
    partial_value = lax.dot_general(
        mixed_out, out_weight, (((0,), (0,)), ((), ())), preferred_element_type=jnp.float32
    )
    branch = lax.psum(partial_value.astype(jnp.bfloat16), "tp").astype(jnp.float32)
    middle = (residual_in.astype(jnp.float32) + branch).astype(jnp.bfloat16)
    middle_wide = middle.astype(jnp.float32)
    row_scale = lax.rsqrt(jnp.mean(middle_wide * middle_wide, axis=1, keepdims=True) + 1e-06)
    normed = (middle_wide * row_scale * norm_gain.astype(jnp.float32)).astype(jnp.bfloat16)
    gate_pre = jnp.dot(
        normed,
        lax.all_gather(gate_weight, "sp", axis=0, tiled=True),
        preferred_element_type=jnp.float32,
    )
    up_pre = jnp.dot(
        normed,
        lax.all_gather(up_weight, "sp", axis=0, tiled=True),
        preferred_element_type=jnp.float32,
    )
    down_whole = lax.all_gather(down_weight, "sp", axis=0, tiled=True)
    hidden = (jax.nn.silu(gate_pre) * up_pre).astype(jnp.bfloat16)
    share = row_count // lax.axis_size("tp")
    channel_out = lax.psum_scatter(
        lax.dot_general(
            hidden, down_whole, (((1,), (1,)), ((), ())), preferred_element_type=jnp.float32
        ).astype(jnp.bfloat16),
        "tp",
        scatter_dimension=0,
        tiled=True,
    ).astype(jnp.float32)
    first_row = lax.axis_index("tp") * share
    own_rows = lax.dynamic_slice_in_dim(middle, first_row, share, 0)
    layer_rows = (own_rows.astype(jnp.float32) + channel_out).astype(jnp.bfloat16)
    return lax.all_gather(layer_rows, "tp", axis=0, tiled=True)


def solution(mesh):
    placed = (
        P("sp", None),
        P("tp", "sp"),
        P("tp", "sp"),
        P("tp", None),
        P("tp", None, None),
        P("tp", None, None),
        P("tp"),
        P("tp", "sp"),
        P("tp", None),
        P(),
        P("sp", "tp"),
        P("sp", "tp"),
        P("sp", "tp"),
    )
    return jax.shard_map(
        on_device, mesh=mesh, in_specs=placed, out_specs=P("sp", None), check_vma=False
    )
```

profile of v0, /device:TPU:25, one launch (start us, length us, event | category | flops | bytes accessed | tf_op | source)
XLA Modules:
  0.0 195.4 jit_solution(4351270999682735000)
XLA Ops:
  0.0 0.0 copy-start.5
  0.0 0.8 fusion
  0.8 0.7 reshape.13.gain_ref
  1.5 1.1 copy.27
  2.6 1.1 copy.28
  3.7 0.2 copy.33.rate_ref
  3.9 0.9 copy.32.taps_ref
  4.8 0.0 copy-done.5
  4.8 0.3 copy.29
  5.2 1.5 copy.30
  6.6 2.2 %copy.31 = bf16[128,2816]{0,1:T(8,128)(2,1)} copy(bf16[128,2816]{1,0:T(8,128)(2,1)} %param.25) | data formatting | bytes 1441792 | tf_op args[12]
  8.9 0.0 copy-start.1
  8.9 0.0 copy-start.2
  8.9 0.0 copy-start.3
  8.9 0.0 copy-start.4
  8.9 1.5 pad_maximum_fusion.packed_ref
  10.4 0.0 copy-done.1
  10.4 0.2 copy-done.2
  10.7 0.1 copy-done.3
  10.8 0.2 copy-done.4
  10.9 122.5 %layer_front.1 = (bf16[3,704,2048]{2,1,0:T(8,128)(2,1)}, bf16[4,256,2048]{2,1,0:T(8,128)(2,1)S(1)}, bf16[256,2048]{1,0:T(8,128)(2,1)S(1)}) custom-call(bf16[1024,256]{1,0:T(8,128)(2,1)S(1)} %copy-done.3, bf16[1024,256]{1,0:T(8,128)(2,1)S(1)} %copy-done.4, f32[1024,256]{1,0:T(8,128)S(1)} %copy-done.1, f32[1024,4]{1,0:T(8,128)S(1)} %copy.32.taps_ref, ...), custom_call_target="tpu_custom_call" | custom-call | tf_op jit(solution)/shard_map/layer_front/pallas_call | solution.py:524
  133.5 0.0 copy-start
  133.5 2.0 %copy-done = bf16[4,256,2048]{2,1,0:T(8,128)(2,1)} copy-done((bf16[4,256,2048]{2,1,0:T(8,128)(2,1)}, bf16[4,256,2048]{2,1,0:T(8,128)(2,1)S(1)}, u32[]{:S(2)}) %copy-start) | copy-done | bytes 4194328
  135.5 59.0 %layer_close.1 = bf16[256,2048]{1,0:T(8,128)(2,1)S(1)} custom-call(bf16[4,256,2048]{2,1,0:T(8,128)(2,1)} %copy-done, bf16[3,704,2048]{2,1,0:T(8,128)(2,1)} %get-tuple-element.9.wide_ref, bf16[256,2048]{1,0:T(8,128)(2,1)S(1)} %get-tuple-element.10.mid_ref), custom_call_target="tpu_custom_call" | custom-call | tf_op jit(solution)/shard_map/layer_close/pallas_call | solution.py:681
  194.5 1.0 copy.35
Async XLA Ops:
  0.0 4.8 %copy-start.5 = (bf16[128,2816]{1,0:T(8,128)(2,1)S(1)}, bf16[128,2816]{1,0:T(8,128)(2,1)}, u32[]{:S(2)}) copy-start(bf16[128,2816]{1,0:T(8,128)(2,1)} %param.23) | copy-start | bytes 2162692
  8.9 1.5 copy-start.1
  8.9 1.8 copy-start.2
  8.9 1.9 copy-start.3
  8.9 2.0 %copy-start.4 = (bf16[1024,256]{1,0:T(8,128)(2,1)S(1)}, bf16[1024,256]{1,0:T(8,128)(2,1)}, u32[]{:S(2)}) copy-start(bf16[1024,256]{1,0:T(8,128)(2,1)} %bg_ref.1) | copy-start | bytes 1572868
  133.5 2.0 %copy-start = (bf16[4,256,2048]{2,1,0:T(8,128)(2,1)}, bf16[4,256,2048]{2,1,0:T(8,128)(2,1)S(1)}, u32[]{:S(2)}) copy-start(bf16[4,256,2048]{2,1,0:T(8,128)(2,1)S(1)} %get-tuple-element.8.tok_ref) | copy-start | bytes 12582916
where the time goes:
time: 196 us; the launch traced here: 195 us
  Pallas kernels  182 us (93%)
  local copies, waits for them, and re-layouts  11.6 us (6%)
  other arithmetic  2.27 us (1%)
    pallas_call x1, Pallas kernels, layer_front(): pl.pallas_call(functools.partial(layer_kernel, n, split), out_shape=(jax....  123 us
    pallas_call x1, Pallas kernels, layer_close(): pl.pallas_call(functools.partial(close_kernel, n, split), out_shape=jax.S...  59 us
    unnamed x18, local copies, waits for them, and re-layouts  9.76 us

commit v1 on v0

v1 whole, which is shorter than its diff:
```python
import functools

import jax
import jax.numpy as jnp
from jax import lax
from jax.experimental import pallas as pl
from jax.experimental.pallas import tpu as pltpu
from jax.sharding import PartitionSpec as P

MESH = pl.DeviceIdType.MESH
LANES = 128


def neg_expm1(v):
    series = jnp.full_like(v, 1.0)
    for k in range(9, 1, -1):
        series = 1.0 + series * v * (1.0 / k)
    return jnp.where(v > -0.5, -v * series, 1.0 - jnp.exp(v))


def mixer_kernel(
    n,
    x_ref,
    halo_ref,
    bg_ref,
    extra_ref,
    taps_ref,
    rate_ref,
    wr_ref,
    wa_ref,
    out_ref,
    state_s,
    run_s,
    ends_s,
    all_s,
    in_s,
    send_sem,
    recv_sem,
):
    me = lax.axis_index("sp")
    barrier = pltpu.get_barrier_semaphore()

    def greet(k, carry):
        pl.semaphore_signal(
            barrier, inc=1, device_id={"sp": lax.rem(me + k, n)}, device_id_type=MESH
        )
        return carry

    lax.fori_loop(1, n, greet, 0)
    channels, length = x_ref.shape
    block = wr_ref.shape[1]
    groups = channels // LANES
    tap_count = taps_ref.shape[1]
    lane = lax.broadcasted_iota(jnp.int32, (LANES, length), 1)

    def local(g, carry):
        rows = pl.ds(pl.multiple_of(g * LANES, LANES), LANES)
        wide = jnp.concatenate(
            [halo_ref[rows, :].astype(jnp.float32), x_ref[rows, :].astype(jnp.float32)], axis=1
        )
        taps = taps_ref[rows, :]
        total = taps[:, tap_count - 1 :] * wide[:, LANES:]
        for tap in range(tap_count - 2, -1, -1):
            total = total + taps[:, tap : tap + 1] * pltpu.roll(wide, tap_count - 1 - tap, 1)[:, LANES:]
        conv = total.astype(jnp.bfloat16)
        per = LANES // block
        recur, admit = [], []
        for b in range(per):
            part = conv[b * block : (b + 1) * block]
            recur.append(jnp.dot(wr_ref[g * per + b], part, preferred_element_type=jnp.float32))
            admit.append(jnp.dot(wa_ref[g * per + b], part, preferred_element_type=jnp.float32))
        recur = jax.nn.sigmoid(jnp.concatenate(recur, axis=0))
        admit = jax.nn.sigmoid(jnp.concatenate(admit, axis=0))
        log_decay = recur * rate_ref[rows, :] + extra_ref[rows, :]
        a = jnp.exp(log_decay)
        b = jnp.sqrt(neg_expm1(2.0 * log_decay)) * admit * conv.astype(jnp.float32)
        shift = 1
        while shift < length:
            seen = lane >= shift
            b = b + a * jnp.where(seen, pltpu.roll(b, shift, 1), 0.0)
            a = a * jnp.where(seen, pltpu.roll(a, shift, 1), 1.0)
            shift *= 2
        state_s[rows, :] = b
        run_s[rows, :] = a
        ends_s[pl.ds(g, 1), :] = a[:, length - LANES :].T[LANES - 1 :]
        ends_s[pl.ds(groups + g, 1), :] = b[:, length - LANES :].T[LANES - 1 :]
        return carry

    lax.fori_loop(0, groups, local, 0)
    pl.semaphore_wait(barrier, n - 1)

    def copy_to(k):
        return pltpu.make_async_remote_copy(
            src_ref=ends_s,
            dst_ref=all_s.at[k - 1],
            send_sem=send_sem.at[k - 1],
            recv_sem=recv_sem.at[k - 1],
            device_id={"sp": lax.rem(me + k, n)},
            device_id_type=MESH,
        )

    def send(k, carry):
        copy_to(k).start()
        return carry

    lax.fori_loop(1, n, send, 0)

    def finish(k, carry):
        copy_to(k).wait()
        return carry

    lax.fori_loop(1, n, finish, 0)

    def fold(i, before):
        k = n - 1 - i
        part = all_s[k - 1]
        new = part[:groups] * before + part[groups:]
        return jnp.where(k <= me, new, before)

    in_s[...] = lax.fori_loop(0, n - 1, fold, jnp.zeros((groups, LANES), jnp.float32))

    def close(g, carry):
        rows = pl.ds(pl.multiple_of(g * LANES, LANES), LANES)
        entering = jnp.broadcast_to(in_s[pl.ds(g, 1), :], (LANES, LANES)).T
        entering = jnp.concatenate([entering] * (length // LANES), axis=1)
        states = state_s[rows, :] + run_s[rows, :] * entering
        v = bg_ref[rows, :].astype(jnp.float32)
        act = 0.5 * v * (1.0 + jnp.tanh(0.7978845608028654 * (v + 0.044715 * v * v * v)))
        out_ref[rows, :] = (states * act).astype(jnp.bfloat16)
        return carry

    lax.fori_loop(0, groups, close, 0)


def mixer(n, x, halo, bg, extra, taps, rate, wr, wa):
    channels, length = x.shape
    groups = channels // LANES
    vmem = pl.BlockSpec(memory_space=pltpu.VMEM)
    return pl.pallas_call(
        functools.partial(mixer_kernel, n),
        out_shape=jax.ShapeDtypeStruct((channels, length), jnp.bfloat16),
        in_specs=[vmem] * 8,
        out_specs=vmem,
        scratch_shapes=[
            pltpu.VMEM((channels, length), jnp.float32),
            pltpu.VMEM((channels, length), jnp.float32),
            pltpu.VMEM((2 * groups, LANES), jnp.float32),
            pltpu.VMEM((n - 1, 2 * groups, LANES), jnp.float32),
            pltpu.VMEM((groups, LANES), jnp.float32),
            pltpu.SemaphoreType.DMA((n - 1,)),
            pltpu.SemaphoreType.DMA((n - 1,)),
        ],
        compiler_params=pltpu.CompilerParams(
            collective_id=0, has_side_effects=True, vmem_limit_bytes=24 << 20
        ),
        cost_estimate=pl.CostEstimate(
            flops=200 * channels * length, bytes_accessed=12 * channels * length, transcendentals=0
        ),
        name="mixer",
    )(x, halo, bg, extra, taps, rate, wr, wa)


def layer_kernel(
    n, split,
    x_ref, bg_ref, extra_ref, taps_ref, dp_ref, wr_ref, wa_ref, ow_ref, res_ref, gain_ref,
    gw_ref, uw_ref, dw_ref,
    out_ref,
    x_s, bg_s, extra_s, ow_s, res_s, raw_s, pack_s,
    xt_s, halo_s, wbd_s, a_s, b_s, ea_s, eb_s, act_s, ends_s, all_s, in_s, mix_s,
    part_s, part_r, mid_s, tok_s, wide_s, hid_s, ff_s, tp_s, red_s, rz_s,
    in_sem, hs_sem, hr_sem, ss_sem, sr_sem,
    zs_sem, zr_sem, ps_sem, pr_sem, fs_sem, fr_sem, rs_sem, rr_sem,
    bs_sem, br_sem, ts_sem, tr_sem, cs_sem, cr_sem,
    as_sem, ar_sem, ks_sem, kr_sem, os_sem, or_sem,
):
    me = lax.axis_index("sp")
    core = lax.axis_index("tp")
    plane = n // split
    rank, spot = me // plane, lax.rem(me, plane)
    f32, bf16 = jnp.float32, jnp.bfloat16
    channels, length = x_s.shape
    groups = channels // LANES
    block = wr_ref.shape[1]
    taps = taps_ref.shape[0]
    kinds, full, depth = pack_s.shape
    span = full // split
    width = mid_s.shape[1]
    barrier = pltpu.get_barrier_semaphore()

    raw_refs = (gw_ref, uw_ref, dw_ref)
    loads = [
        pltpu.make_async_copy(src, dst, in_sem.at[i])
        for i, (src, dst) in enumerate(
            [
                (x_ref, x_s),
                (gw_ref, raw_s.at[0]),
                (uw_ref, raw_s.at[1]),
                (dw_ref, raw_s.at[2]),
                (extra_ref, extra_s),
                (bg_ref, bg_s),
                (ow_ref, ow_s),
                (res_ref, res_s),
            ]
        )
    ]
    for load in loads:
        load.start()

    def greet(k, carry):
        pl.semaphore_signal(
            barrier, inc=1, device_id={"sp": lax.rem(me + k, n)}, device_id_type=MESH
        )
        return carry

    lax.fori_loop(1, n, greet, 0)
    pl.semaphore_signal(barrier, inc=1, device_id={"tp": 1 - core}, device_id_type=MESH)

    def remote(src, dst, ssem, rsem, where):
        return pltpu.make_async_remote_copy(
            src_ref=src, dst_ref=dst, send_sem=ssem, recv_sem=rsem,
            device_id=where, device_id_type=MESH,
        )

    def lanes(i):
        return pl.ds(pl.multiple_of(i * LANES, LANES), LANES)

    def own(c):
        return pack_s.at[c, pl.ds(pl.multiple_of(rank * span, span), span)]

    def window(c, source):
        return wide_s.at[c, :, lanes(source)]

    def z_copy(c, k):
        to = lax.rem(rank + k, split)
        return remote(
            pack_s.at[c, pl.ds(pl.multiple_of(to * span, span), span)], window(c, me),
            zs_sem.at[c, k - 1], zr_sem.at[c, k - 1], {"sp": to * plane + spot},
        )

    def from_rank(k):
        return lax.rem(rank - k + split, split)

    def z_landed(c, k):
        source = from_rank(k) * plane + spot
        return remote(
            own(c), window(c, source), zs_sem.at[c, k - 1], zr_sem.at[c, k - 1], {"sp": source}
        )

    def beside(m):
        return spot + 1 - 2 * lax.rem(spot, 2) if m == 1 else spot + 2 - 4 * (spot // 2)

    def pass_copy(c, k, m):
        source = from_rank(k) * plane + spot
        return remote(
            window(c, source) if k else own(c), window(c, source),
            fs_sem.at[c, k, m - 1], fr_sem.at[c, k, m - 1], {"sp": rank * plane + beside(m)},
        )

    def pass_landed(c, k, m):
        source = from_rank(k) * plane + beside(m)
        return remote(
            window(c, source), window(c, source),
            fs_sem.at[c, k, m - 1], fr_sem.at[c, k, m - 1], {"sp": rank * plane + beside(m)},
        )

    def relay_window(c, k, m, where):
        source = from_rank(k) * plane + where
        return wide_s.at[c, pl.ds((m - 1) * (span // 2), span // 2), lanes(source)]

    def relay_copy(c, k, m):
        view = relay_window(c, k, m, beside(m))
        return remote(
            view, view, rs_sem.at[c, k, m - 1], rr_sem.at[c, k, m - 1],
            {"sp": rank * plane + beside(3 - m)},
        )

    def relay_landed(c, k, m):
        view = relay_window(c, k, m, 3 - spot)
        return remote(
            view, view, rs_sem.at[c, k, m - 1], rr_sem.at[c, k, m - 1],
            {"sp": rank * plane + beside(3 - m)},
        )

    def z_start(c):
        for k in range(1, split):
            z_copy(c, k).start()

    def spread(c, k):
        if k:
            z_landed(c, k).wait_recv()
        for m in (1, 2):
            pass_copy(c, k, m).start()

    def relay(c, k):
        for m in (1, 2):
            pass_landed(c, k, m).wait_recv()
            relay_copy(c, k, m).start()

    def settle(c):
        for k in range(split):
            for m in (1, 2):
                relay_landed(c, k, m).wait_recv()

    def turn(c):
        loads[1 + c].wait()

        def step(j, carry):
            pack_s[c, lanes(j), :] = raw_s[c, :, lanes(j)].T
            return carry

        lax.fori_loop(0, full // LANES, step, 0)

    def keep(c):
        wide_s[c, :, lanes(me)] = own(c)[...]

    loads[0].wait()

    def flip(g, carry):
        xt_s[pl.ds(8, length), lanes(g)] = x_s[lanes(g), :].astype(f32).T
        return carry

    lax.fori_loop(0, groups, flip, 0)
    turn(0)
    pl.semaphore_wait(barrier, n)
    halo = remote(
        xt_s.at[pl.ds(length, 8), :], halo_s, hs_sem, hr_sem, {"sp": lax.rem(me + 1, n)}
    )
    halo.start()
    z_start(0)
    spread(0, 0)
    turn(1)
    spread(1, 0)
    turn(2)
    spread(2, 0)
    for c in range(kinds):
        keep(c)

    rowb = lax.broadcasted_iota(jnp.int32, (LANES, LANES), 0) // block
    colb = lax.broadcasted_iota(jnp.int32, (LANES, LANES), 1) // block
    eye_r = lax.broadcasted_iota(jnp.int32, (block, LANES), 0)
    eye_c = lax.rem(lax.broadcasted_iota(jnp.int32, (block, LANES), 1), block)
    twice = jnp.where(eye_r == eye_c, 1.0, 0.0).astype(bf16)

    def widen(g, carry):
        for slot, w_ref in ((0, wr_ref), (1, wa_ref)):
            pair = jnp.concatenate([w_ref[2 * g], w_ref[2 * g + 1]], axis=0)
            both = jnp.dot(pair, twice, preferred_element_type=f32)
            wbd_s[g, :, slot * LANES : (slot + 1) * LANES] = jnp.where(
                rowb == colb, both, 0.0
            ).astype(bf16)
        return carry

    lax.fori_loop(0, groups, widen, 0)
    loads[4].wait()
    halo.wait()
    xt_s[0:8, :] = halo_s[...] * jnp.where(me > 0, 1.0, 0.0)

    octets = length // 8
    sub = lax.broadcasted_iota(jnp.int32, (octets, 8, LANES), 1)
    row = lax.broadcasted_iota(jnp.int32, (octets, LANES), 0)

    def local(g, carry):
        cols = lanes(g)
        tap = taps_ref[:, cols].astype(f32)
        total = tap[taps - 1 : taps] * xt_s[pl.ds(8, length), cols]
        for k in range(taps - 2, -1, -1):
            total = total + tap[k : k + 1] * xt_s[pl.ds(9 - taps + k, length), cols]
        conv = total.astype(bf16)
        both = jnp.dot(conv, wbd_s[g], preferred_element_type=f32)
        recur = jax.nn.sigmoid(both[:, :LANES])
        admit = jax.nn.sigmoid(both[:, LANES:])
        rate = -8.0 * jax.nn.softplus(-dp_ref[pl.ds(g, 1), :])
        log_decay = recur * rate + extra_s[lanes(g), :].T
        a = jnp.exp(log_decay)
        b = jnp.sqrt(neg_expm1(2.0 * log_decay)) * admit * conv.astype(f32)
        a = a.reshape(octets, 8, LANES)
        b = b.reshape(octets, 8, LANES)
        for shift in (1, 2, 4):
            seen = sub >= shift
            b = b + a * jnp.where(seen, pltpu.roll(b, shift, 1), 0.0)
            a = a * jnp.where(seen, pltpu.roll(a, shift, 1), 1.0)
        a_s[g] = a.reshape(length, LANES)
        b_s[g] = b.reshape(length, LANES)
        ea = a_s[g, pl.ds(7, octets, stride=8), :]
        eb = b_s[g, pl.ds(7, octets, stride=8), :]
        shift = 1
        while shift < octets:
            seen = row >= shift
            eb = eb + ea * jnp.where(seen, pltpu.roll(eb, shift, 0), 0.0)
            ea = ea * jnp.where(seen, pltpu.roll(ea, shift, 0), 1.0)
            shift *= 2
        ends_s[pl.ds(g, 1), :] = ea[octets - 1 :]
        ends_s[pl.ds(groups + g, 1), :] = eb[octets - 1 :]
        ea_s[g] = jnp.where(row >= 1, pltpu.roll(ea, 1, 0), 1.0)
        eb_s[g] = jnp.where(row >= 1, pltpu.roll(eb, 1, 0), 0.0)
        return carry

    lax.fori_loop(0, groups, local, 0)

    def state(k):
        return remote(
            ends_s, all_s.at[k - 1], ss_sem.at[k - 1], sr_sem.at[k - 1],
            {"sp": lax.rem(me + k, n)},
        )

    def state_send(k, carry):
        state(k).start()
        return carry

    lax.fori_loop(1, n, state_send, 0)
    for c in range(kinds):
        relay(c, 0)
    for k in range(1, split):
        spread(0, k)
    z_start(1)
    loads[5].wait()

    def gelu(g, carry):
        v = bg_s[lanes(g), :].astype(f32).T
        act_s[g] = 0.5 * v * (1.0 + jnp.tanh(0.7978845608028654 * (v + 0.044715 * v * v * v)))
        return carry

    lax.fori_loop(0, groups, gelu, 0)

    def state_wait(k, carry):
        state(k).wait()
        return carry

    lax.fori_loop(1, n, state_wait, 0)

    def fold(i, before):
        k = n - 1 - i
        part = all_s[k - 1]
        new = part[:groups] * before + part[groups:]
        return jnp.where(k <= me, new, before)

    in_s[...] = lax.fori_loop(0, n - 1, fold, jnp.zeros((groups, LANES), f32))

    def close(g, carry):
        enter = eb_s[g] + ea_s[g] * in_s[pl.ds(g, 1), :]
        states = jnp.concatenate(
            [
                b_s[g, i * 8 : i * 8 + 8, :] + a_s[g, i * 8 : i * 8 + 8, :] * enter[i : i + 1]
                for i in range(octets)
            ],
            axis=0,
        )
        mix_s[:, lanes(g)] = (states * act_s[g]).astype(bf16)
        return carry

    lax.fori_loop(0, groups, close, 0)

    pieces, row_count, cut = part_s.shape

    def swap(i):
        return remote(
            part_s.at[i], part_r.at[i], bs_sem.at[i], br_sem.at[i], {"tp": 1 - core}
        )

    loads[6].wait()
    for i in range(pieces):
        part_s[i] = jnp.dot(
            mix_s[...], ow_s[:, i * cut : (i + 1) * cut], preferred_element_type=f32
        ).astype(bf16)
        swap(i).start()
    for k in range(1, split):
        relay(0, k)
    loads[7].wait()
    square = jnp.zeros((row_count, 1), f32)
    for i in range(pieces):
        swap(i).wait()
        cols = slice(i * cut, (i + 1) * cut)
        branch = part_s[i].astype(f32) + part_r[i].astype(f32)
        middle = (res_s[:, cols].astype(f32) + branch).astype(bf16)
        mid_s[:, cols] = middle
        middle = middle.astype(f32)
        square = square + jnp.sum(middle * middle, axis=1, keepdims=True)
    scale = lax.rsqrt(square * (1.0 / (pieces * cut)) + 1e-06)
    for i in range(width // LANES):
        cols = slice(i * LANES, (i + 1) * LANES)
        gain = gain_ref[i : i + 1, :].astype(f32)
        tok_s[rank, :, cols] = (mid_s[:, cols].astype(f32) * scale * gain).astype(bf16)

    half = row_count // 2
    mine = pl.ds(pl.multiple_of(core * half, half), half)
    other = pl.ds(pl.multiple_of((1 - core) * half, half), half)

    def tok_copy(way, d):
        step = 1 - 2 * way
        view = tok_s.at[rank - (d - 1) * step, mine, :]
        return remote(
            view, view, ts_sem.at[way, d - 1], tr_sem.at[way, d - 1],
            {"sp": (rank + step) * plane + spot},
        )

    def tok_landed(way, d):
        step = 1 - 2 * way
        view = tok_s.at[rank - d * step, mine, :]
        return remote(
            view, view, ts_sem.at[way, d - 1], tr_sem.at[way, d - 1],
            {"sp": (rank - step) * plane + spot},
        )

    def tok_pass(way, d, rows):
        view = tok_s.at[rank - d * (1 - 2 * way), rows, :]
        return remote(
            view, view, cs_sem.at[way, d - 1], cr_sem.at[way, d - 1], {"tp": 1 - core}
        )

    def held(way, d):
        return rank >= d if way == 0 else rank <= split - 1 - d

    def onward(way, d):
        return (
            jnp.logical_and(rank >= d, rank < split - 1)
            if way == 0
            else jnp.logical_and(rank <= split - 1 - d, rank > 0)
        )

    for way in (0, 1):

        @pl.when(onward(way, 0))
        def _():
            tok_copy(way, 1).start()

    def tok_relay(d):
        for way in (0, 1):

            @pl.when(held(way, d))
            def _():
                tok_landed(way, d).wait_recv()
                tok_pass(way, d, mine).start()

            if d < split - 1:

                @pl.when(onward(way, d))
                def _():
                    tok_copy(way, d + 1).start()

    def tok_ready(d):
        for way in (0, 1):

            @pl.when(held(way, d))
            def _():
                tok_pass(way, d, other).wait_recv()

    z_start(2)
    for k in range(1, split):
        spread(1, k)
    for k in range(1, split):
        relay(1, k)
    tok_relay(1)
    settle(0)
    settle(1)
    for k in range(1, split):
        spread(2, k)
    tok_relay(2)
    for k in range(1, split):
        relay(2, k)
    tok_relay(3)
    settle(2)
    for d in range(1, split):
        tok_ready(d)

    side = rank // 2
    inner = lax.rem(rank, 2) + side - 2 * lax.rem(rank, 2) * side
    chunks, _, chunk = ff_s.shape[1:]
    across = (((1,), (1,)), ((), ()))

    def target(i):
        t = (3, 2, 1 - inner, inner)[i]
        return t + side * (split - 1 - 2 * t)

    def feed(i):
        tokens = tok_s[target(i)]
        gate = lax.dot_general(tokens, wide_s[0], across, preferred_element_type=f32)
        up = lax.dot_general(tokens, wide_s[1], across, preferred_element_type=f32)
        hid_s[...] = (gate / (1.0 + jnp.exp(-gate)) * up).astype(bf16)
        for q in range(chunks):
            ff_s[i, q] = jnp.dot(
                hid_s[...], wide_s[2, :, q * chunk : (q + 1) * chunk], preferred_element_type=f32
            ).astype(bf16)
            tp_copy(i, q).start()

    def tp_copy(i, q):
        return remote(
            ff_s.at[i, q, other, :], tp_s.at[i, q], as_sem.at[i, q], ar_sem.at[i, q],
            {"tp": 1 - core},
        )

    mate = rank + 1 - 2 * lax.rem(rank, 2)
    ahead = rank + 1 - 2 * side

    def sum_copy(i, q):
        slot = i + 3 * inner if i < 2 else 2 + inner
        to = ahead if i < 2 else mate
        return remote(
            red_s.at[i, q], rz_s.at[slot, q], ks_sem.at[i, q], kr_sem.at[slot, q],
            {"sp": to * plane + spot},
        )

    def sum_landed(slot, q):
        return remote(
            red_s.at[0, q], rz_s.at[slot, q], ks_sem.at[0, q], kr_sem.at[slot, q],
            {"sp": mate * plane + spot},
        )

    def pair(i, q):
        tp_copy(i, q).wait()
        return ff_s[i, q, mine, :].astype(f32) + tp_s[i, q].astype(f32)

    def push(i, q):
        slot = i if i < 2 else 3

        @pl.when(inner == 0)
        def _():
            red_s[i, q] = pair(i, q).astype(bf16)

        @pl.when(inner == 1)
        def _():
            mixed = pair(i, q)
            sum_landed(slot, q).wait_recv()
            red_s[i, q] = (mixed + rz_s[slot, q].astype(f32)).astype(bf16)

        sum_copy(i, q).start()

    def out_copy(q):
        view = out_ref.at[mine, pl.ds(q * chunk, chunk)]
        return remote(view, view, os_sem.at[q], or_sem.at[q], {"tp": 1 - core})

    def out_landed(q):
        view = out_ref.at[other, pl.ds(q * chunk, chunk)]
        return remote(view, view, os_sem.at[q], or_sem.at[q], {"tp": 1 - core})

    def finish(q):
        cols = slice(q * chunk, (q + 1) * chunk)
        i = split - 1
        base = mid_s[mine, cols].astype(f32)

        @pl.when(inner == 0)
        def _():
            mixed = pair(i, q)
            sum_landed(3, q).wait_recv()
            out_ref[mine, cols] = (base + (mixed + rz_s[3, q].astype(f32))).astype(bf16)

        @pl.when(inner == 1)
        def _():
            mixed = pair(i, q)
            sum_landed(2, q).wait_recv()
            mixed = mixed + rz_s[2, q].astype(f32)
            sum_landed(4, q).wait_recv()
            out_ref[mine, cols] = (base + (mixed + rz_s[4, q].astype(f32))).astype(bf16)

        out_copy(q).start()

    feed(0)
    feed(1)
    for q in range(chunks):
        push(0, q)
    feed(2)
    for q in range(chunks):
        push(1, q)
    feed(3)
    for q in range(chunks):
        push(2, q)
    for q in range(chunks):
        finish(q)

    for q in range(chunks):
        out_copy(q).wait_send()
        out_landed(q).wait_recv()
        for i in range(split - 1):
            sum_copy(i, q).wait_send()
    for way in (0, 1):
        for d in range(1, split):

            @pl.when(onward(way, d - 1))
            def _():
                tok_copy(way, d).wait_send()

            @pl.when(held(way, d))
            def _():
                tok_pass(way, d, mine).wait_send()

    for c in range(kinds):
        for k in range(split):
            for m in (1, 2):
                pass_copy(c, k, m).wait_send()
                relay_copy(c, k, m).wait_send()
            if k:
                z_copy(c, k).wait_send()


def layer(n, split, x, bg, extra, taps, dp, wr, wa, ow, res, gain, gw, uw, dw):
    channels, length = x.shape
    groups = channels // LANES
    rows, width = res.shape
    depth, full = gw.shape
    span = full // split
    kinds = 3
    cut = 512
    pieces = width // cut
    chunk = width // 2
    chunks = width // chunk
    half = rows // 2
    vmem = pl.BlockSpec(memory_space=pltpu.VMEM)
    hbm = pl.BlockSpec(memory_space=pl.ANY)
    dma = pltpu.SemaphoreType.DMA
    bf16, f32 = jnp.bfloat16, jnp.float32
    buf = pltpu.VMEM
    return pl.pallas_call(
        functools.partial(layer_kernel, n, split),
        out_shape=jax.ShapeDtypeStruct((rows, width), bf16),
        in_specs=[hbm, hbm, hbm, vmem, vmem, vmem, vmem, hbm, hbm, vmem, hbm, hbm, hbm],
        out_specs=vmem,
        scratch_shapes=[
            buf((channels, length), bf16),
            buf((channels, length), bf16),
            buf((channels, length), f32),
            buf((channels, width), bf16),
            buf((rows, width), bf16),
            buf((kinds, depth, full), bf16),
            buf((kinds, full, depth), bf16),
            buf((length + 8, channels), f32),
            buf((8, channels), f32),
            buf((groups, LANES, 2 * LANES), bf16),
            buf((groups, length, LANES), f32),
            buf((groups, length, LANES), f32),
            buf((groups, length // 8, LANES), f32),
            buf((groups, length // 8, LANES), f32),
            buf((groups, length, LANES), f32),
            buf((2 * groups, LANES), f32),
            buf((n - 1, 2 * groups, LANES), f32),
            buf((groups, LANES), f32),
            buf((length, channels), bf16),
            buf((pieces, rows, cut), bf16),
            buf((pieces, rows, cut), bf16),
            buf((rows, width), bf16),
            buf((split, rows, width), bf16),
            buf((kinds, span, width), bf16),
            buf((rows, span), bf16),
            buf((split, chunks, rows, chunk), bf16),
            buf((split, chunks, half, chunk), bf16),
            buf((split - 1, chunks, half, chunk), bf16),
            buf((5, chunks, half, chunk), bf16),
            dma((8,)),
            dma,
            dma,
            dma((n - 1,)),
            dma((n - 1,)),
            dma((kinds, split - 1)),
            dma((kinds, split - 1)),
            dma((1,)),
            dma((1,)),
            dma((kinds, split, 2)),
            dma((kinds, split, 2)),
            dma((kinds, split, 2)),
            dma((kinds, split, 2)),
            dma((pieces,)),
            dma((pieces,)),
            dma((2, split - 1)),
            dma((2, split - 1)),
            dma((2, split - 1)),
            dma((2, split - 1)),
            dma((split, chunks)),
            dma((split, chunks)),
            dma((split - 1, chunks)),
            dma((5, chunks)),
            dma((chunks,)),
            dma((chunks,)),
        ],
        compiler_params=pltpu.CompilerParams(
            collective_id=1, has_side_effects=True, vmem_limit_bytes=60 << 20
        ),
        name="layer",
    )(x, bg, extra, taps, dp, wr, wa, ow, res, gain, gw, uw, dw)


def on_device(
    residual_in,
    mixer_input,
    branch_gate,
    conv_taps,
    recur_weight,
    admit_weight,
    decay_param,
    decay_extra,
    out_weight,
    norm_gain,
    gate_weight,
    up_weight,
    down_weight,
):
    n = lax.axis_size("sp")
    length = mixer_input.shape[1]
    width, share_ff = residual_in.shape[1], gate_weight.shape[1]
    split = 4
    depth = gate_weight.shape[0]
    if (
        lax.axis_size("tp") == 2
        and n == 4 * split
        and depth == LANES
        and width == n * depth
        and share_ff % LANES == 0
        and share_ff % (32 * split) == 0
        and 2 * recur_weight.shape[1] == LANES
        and conv_taps.shape[1] <= 9
        and residual_in.shape[0] == length
        and length % (2 * LANES) == 0
    ):
        return layer(
            n,
            split,
            mixer_input,
            branch_gate,
            decay_extra,
            conv_taps.T,
            decay_param.reshape(-1, LANES),
            recur_weight,
            admit_weight,
            out_weight,
            residual_in,
            norm_gain.reshape(-1, LANES),
            gate_weight,
            up_weight,
            down_weight,
        )
    halo = lax.ppermute(
        mixer_input[:, length - LANES :], "sp", [(i, i + 1) for i in range(n - 1)]
    )
    rate = -8.0 * jax.nn.softplus(-decay_param)[:, None]
    mixed_out = mixer(
        n,
        mixer_input,
        halo,
        branch_gate,
        decay_extra,
        conv_taps.astype(jnp.float32),
        rate,
        recur_weight.transpose(0, 2, 1),
        admit_weight.transpose(0, 2, 1),
    )
    row_count = residual_in.shape[0]
    partial_value = lax.dot_general(
        mixed_out, out_weight, (((0,), (0,)), ((), ())), preferred_element_type=jnp.float32
    )
    branch = lax.psum(partial_value.astype(jnp.bfloat16), "tp").astype(jnp.float32)
    middle = (residual_in.astype(jnp.float32) + branch).astype(jnp.bfloat16)
    middle_wide = middle.astype(jnp.float32)
    row_scale = lax.rsqrt(jnp.mean(middle_wide * middle_wide, axis=1, keepdims=True) + 1e-06)
    normed = (middle_wide * row_scale * norm_gain.astype(jnp.float32)).astype(jnp.bfloat16)
    gate_pre = jnp.dot(
        normed,
        lax.all_gather(gate_weight, "sp", axis=0, tiled=True),
        preferred_element_type=jnp.float32,
    )
    up_pre = jnp.dot(
        normed,
        lax.all_gather(up_weight, "sp", axis=0, tiled=True),
        preferred_element_type=jnp.float32,
    )
    down_whole = lax.all_gather(down_weight, "sp", axis=0, tiled=True)
    hidden = (jax.nn.silu(gate_pre) * up_pre).astype(jnp.bfloat16)
    share = row_count // lax.axis_size("tp")
    channel_out = lax.psum_scatter(
        lax.dot_general(
            hidden, down_whole, (((1,), (1,)), ((), ())), preferred_element_type=jnp.float32
        ).astype(jnp.bfloat16),
        "tp",
        scatter_dimension=0,
        tiled=True,
    ).astype(jnp.float32)
    first_row = lax.axis_index("tp") * share
    own_rows = lax.dynamic_slice_in_dim(middle, first_row, share, 0)
    layer_rows = (own_rows.astype(jnp.float32) + channel_out).astype(jnp.bfloat16)
    return lax.all_gather(layer_rows, "tp", axis=0, tiled=True)


def solution(mesh):
    placed = (
        P("sp", None),
        P("tp", "sp"),
        P("tp", "sp"),
        P("tp", None),
        P("tp", None, None),
        P("tp", None, None),
        P("tp"),
        P("tp", "sp"),
        P("tp", None),
        P(),
        P("sp", "tp"),
        P("sp", "tp"),
        P("sp", "tp"),
    )
    return jax.shard_map(
        on_device, mesh=mesh, in_specs=placed, out_specs=P("sp", None), check_vma=False
    )
```

time: 196 us -> 146 us (0.74)
  the two profiles are of different devices: /device:TPU:25 before, /device:TPU:0 now
where the time goes in v1:
time: 146 us; the launch traced here: 144 us
  Pallas kernels  142 us (97%)
  local copies, waits for them, and re-layouts  2.3 us (2%)
    pallas_call x1, Pallas kernels, layer(): pl.pallas_call(functools.partial(layer_kernel, n, split), out_shape=jax.S...  142 us

profile of v1, /device:TPU:0, one launch (start us, length us, event | category | flops | bytes accessed | tf_op | source)
XLA Modules:
  0.0 144.4 jit_solution(12686505278495574038)
XLA Ops:
  0.0 142.1 %layer.1 = bf16[256,2048]{1,0:T(8,128)(2,1)} custom-call(bf16[1024,256]{1,0:T(8,128)(2,1)} %x_ref.1, bf16[1024,256]{1,0:T(8,128)(2,1)} %bg_ref.1, f32[1024,256]{1,0:T(8,128)} %extra_ref.1, bf16[4,1024]{1,0:T(4,128)(2,1)} %bitcast.3, f32[8,128]{1,0:T(8,128)} %bitcast.4, bf16[16,64,64]{2,1,0:T(8,128)(2,1)} %wr_ref.1, bf16[16,64,64]{2,1,0:T(8,128)(2,1)} %wa_ref.1, ...), custom_call_target="tpu_custom_call" | custom-call | tf_op jit(solution)/shard_map/layer/pallas_call | solution.py:711
  142.1 2.3 %copy.15 = bf16[256,2048]{1,0:T(8,128)(2,1)} copy(bf16[256,2048]{1,0:T(8,128)(2,1)} %layer.1) | data formatting | bytes 2097152

commit v2 on v1

--- a/solution.py
+++ b/solution.py
@@ -230,18 +230,29 @@
     def window(c, source):
         return wide_s.at[c, :, lanes(source)]
 
+    side = rank // 2
+    inner = lax.rem(rank, 2) + side - 2 * lax.rem(rank, 2) * side
+    mate = rank + 1 - 2 * lax.rem(rank, 2)
+    ahead = rank + 1 - 2 * side
+
+    def away(k):
+        if k < 2:
+            return (rank, mate)[k]
+        t = 2 if k == 2 else 3
+        return t + side * (split - 1 - 2 * t)
+
+    def there(k):
+        return k if k < 2 else 3 - inner
+
     def z_copy(c, k):
-        to = lax.rem(rank + k, split)
+        to = away(k)
         return remote(
             pack_s.at[c, pl.ds(pl.multiple_of(to * span, span), span)], window(c, me),
-            zs_sem.at[c, k - 1], zr_sem.at[c, k - 1], {"sp": to * plane + spot},
-        )
-
-    def from_rank(k):
-        return lax.rem(rank - k + split, split)
+            zs_sem.at[c, k - 1], zr_sem.at[c, there(k) - 1], {"sp": to * plane + spot},
+        )
 
     def z_landed(c, k):
-        source = from_rank(k) * plane + spot
+        source = away(k) * plane + spot
         return remote(
             own(c), window(c, source), zs_sem.at[c, k - 1], zr_sem.at[c, k - 1], {"sp": source}
         )
@@ -250,21 +261,21 @@
         return spot + 1 - 2 * lax.rem(spot, 2) if m == 1 else spot + 2 - 4 * (spot // 2)
 
     def pass_copy(c, k, m):
-        source = from_rank(k) * plane + spot
+        source = away(k) * plane + spot
         return remote(
             window(c, source) if k else own(c), window(c, source),
             fs_sem.at[c, k, m - 1], fr_sem.at[c, k, m - 1], {"sp": rank * plane + beside(m)},
         )
 
     def pass_landed(c, k, m):
-        source = from_rank(k) * plane + beside(m)
+        source = away(k) * plane + beside(m)
         return remote(
             window(c, source), window(c, source),
             fs_sem.at[c, k, m - 1], fr_sem.at[c, k, m - 1], {"sp": rank * plane + beside(m)},
         )
 
     def relay_window(c, k, m, where):
-        source = from_rank(k) * plane + where
+        source = away(k) * plane + where
         return wide_s.at[c, pl.ds((m - 1) * (span // 2), span // 2), lanes(source)]
 
     def relay_copy(c, k, m):
@@ -282,8 +293,17 @@
         )
 
     def z_start(c):
-        for k in range(1, split):
+        @pl.when(inner == 0)
+        def _():
+            z_copy(c, 1).start()
+
+        for k in range(2, split):
             z_copy(c, k).start()
+
+    def z_mate(c):
+        @pl.when(inner == 1)
+        def _():
+            z_copy(c, 1).start()
 
     def spread(c, k):
         if k:
@@ -296,10 +316,9 @@
             pass_landed(c, k, m).wait_recv()
             relay_copy(c, k, m).start()
 
-    def settle(c):
-        for k in range(split):
-            for m in (1, 2):
-                relay_landed(c, k, m).wait_recv()
+    def settle(c, k):
+        for m in (1, 2):
+            relay_landed(c, k, m).wait_recv()
 
     def turn(c):
         loads[1 + c].wait()
@@ -326,12 +345,12 @@
         xt_s.at[pl.ds(length, 8), :], halo_s, hs_sem, hr_sem, {"sp": lax.rem(me + 1, n)}
     )
     halo.start()
+    z_mate(0)
     z_start(0)
     spread(0, 0)
     turn(1)
     spread(1, 0)
     turn(2)
-    spread(2, 0)
     for c in range(kinds):
         keep(c)
 
@@ -407,12 +426,12 @@
         state(k).start()
         return carry
 
-    lax.fori_loop(1, n, state_send, 0)
-    for c in range(kinds):
-        relay(c, 0)
-    for k in range(1, split):
-        spread(0, k)
+    lax.fori_loop(1, n - me, state_send, 0)
     z_start(1)
+    z_start(2)
+    spread(0, 1)
+    relay(0, 0)
+    spread(2, 0)
     loads[5].wait()
 
     def gelu(g, carry):
@@ -421,20 +440,33 @@
         return carry
 
     lax.fori_loop(0, groups, gelu, 0)
+    relay(1, 0)
+    z_mate(1)
+    spread(0, 2)
+    relay(0, 1)
+    spread(0, 3)
+    relay(2, 0)
+    z_mate(2)
+    spread(1, 1)
 
     def state_wait(k, carry):
-        state(k).wait()
-        return carry
-
-    lax.fori_loop(1, n, state_wait, 0)
+        remote(
+            ends_s, all_s.at[k - 1], ss_sem.at[k - 1], sr_sem.at[k - 1],
+            {"sp": lax.rem(me - k + n, n)},
+        ).wait_recv()
+        return carry
+
+    lax.fori_loop(1, me + 1, state_wait, 0)
+
+    def state_sent(k, carry):
+        state(k).wait_send()
+        return carry
 
     def fold(i, before):
-        k = n - 1 - i
-        part = all_s[k - 1]
-        new = part[:groups] * before + part[groups:]
-        return jnp.where(k <= me, new, before)
-
-    in_s[...] = lax.fori_loop(0, n - 1, fold, jnp.zeros((groups, LANES), f32))
+        part = all_s[me - 1 - i]
+        return part[:groups] * before + part[groups:]
+
+    in_s[...] = lax.fori_loop(0, me, fold, jnp.zeros((groups, LANES), f32))
 
     def close(g, carry):
         enter = eb_s[g] + ea_s[g] * in_s[pl.ds(g, 1), :]
@@ -463,8 +495,7 @@
             mix_s[...], ow_s[:, i * cut : (i + 1) * cut], preferred_element_type=f32
         ).astype(bf16)
         swap(i).start()
-    for k in range(1, split):
-        relay(0, k)
+    relay(0, 2)
     loads[7].wait()
     square = jnp.zeros((row_count, 1), f32)
     for i in range(pieces):
@@ -485,26 +516,32 @@
     mine = pl.ds(pl.multiple_of(core * half, half), half)
     other = pl.ds(pl.multiple_of((1 - core) * half, half), half)
 
-    def tok_copy(way, d):
+    bits = ts_sem.shape[2]
+    bit = half // bits
+
+    def some(which, p):
+        return pl.ds(pl.multiple_of(which * half + p * bit, bit), bit)
+
+    def tok_copy(way, d, p):
         step = 1 - 2 * way
-        view = tok_s.at[rank - (d - 1) * step, mine, :]
-        return remote(
-            view, view, ts_sem.at[way, d - 1], tr_sem.at[way, d - 1],
+        view = tok_s.at[rank - (d - 1) * step, some(core, p), :]
+        return remote(
+            view, view, ts_sem.at[way, d - 1, p], tr_sem.at[way, d - 1, p],
             {"sp": (rank + step) * plane + spot},
         )
 
-    def tok_landed(way, d):
+    def tok_landed(way, d, p):
         step = 1 - 2 * way
-        view = tok_s.at[rank - d * step, mine, :]
-        return remote(
-            view, view, ts_sem.at[way, d - 1], tr_sem.at[way, d - 1],
+        view = tok_s.at[rank - d * step, some(core, p), :]
+        return remote(
+            view, view, ts_sem.at[way, d - 1, p], tr_sem.at[way, d - 1, p],
             {"sp": (rank - step) * plane + spot},
         )
 
-    def tok_pass(way, d, rows):
-        view = tok_s.at[rank - d * (1 - 2 * way), rows, :]
-        return remote(
-            view, view, cs_sem.at[way, d - 1], cr_sem.at[way, d - 1], {"tp": 1 - core}
+    def tok_pass(way, d, p, which):
+        view = tok_s.at[rank - d * (1 - 2 * way), some(which, p), :]
+        return remote(
+            view, view, cs_sem.at[way, d - 1, p], cr_sem.at[way, d - 1, p], {"tp": 1 - core}
         )
 
     def held(way, d):
@@ -517,70 +554,67 @@
             else jnp.logical_and(rank <= split - 1 - d, rank > 0)
         )
 
-    for way in (0, 1):
-
-        @pl.when(onward(way, 0))
-        def _():
-            tok_copy(way, 1).start()
-
-    def tok_relay(d):
+    def tok_start():
         for way in (0, 1):
 
-            @pl.when(held(way, d))
+            @pl.when(onward(way, 0))
             def _():
-                tok_landed(way, d).wait_recv()
-                tok_pass(way, d, mine).start()
+                for p in range(bits):
+                    tok_copy(way, 1, p).start()
+
+    def tok_relay(d, close, p):
+        for way in (0, 1):
+            here = lax.rem(rank, 2) == (1 - way if close else way)
+
+            @pl.when(jnp.logical_and(held(way, d), here))
+            def _():
+                tok_landed(way, d, p).wait_recv()
+                tok_pass(way, d, p, core).start()
 
             if d < split - 1:
 
-                @pl.when(onward(way, d))
+                @pl.when(jnp.logical_and(onward(way, d), here))
                 def _():
-                    tok_copy(way, d + 1).start()
-
-    def tok_ready(d):
+                    tok_copy(way, d + 1, p).start()
+
+    def tok_ready(d, close):
         for way in (0, 1):
-
-            @pl.when(held(way, d))
+            here = lax.rem(rank, 2) == (1 - way if close else way)
+
+            @pl.when(jnp.logical_and(held(way, d), here))
             def _():
-                tok_pass(way, d, other).wait_recv()
-
-    z_start(2)
-    for k in range(1, split):
-        spread(1, k)
-    for k in range(1, split):
-        relay(1, k)
-    tok_relay(1)
-    settle(0)
-    settle(1)
-    for k in range(1, split):
-        spread(2, k)
-    tok_relay(2)
-    for k in range(1, split):
-        relay(2, k)
-    tok_relay(3)
-    settle(2)
-    for d in range(1, split):
-        tok_ready(d)
-
-    side = rank // 2
-    inner = lax.rem(rank, 2) + side - 2 * lax.rem(rank, 2) * side
+                for p in range(bits):
+                    tok_pass(way, d, p, 1 - core).wait_recv()
+
     chunks, _, chunk = ff_s.shape[1:]
     across = (((1,), (1,)), ((), ()))
 
     def target(i):
-        t = (3, 2, 1 - inner, inner)[i]
+        t = (1 + inner, 2 - 2 * inner, 3, inner)[i]
         return t + side * (split - 1 - 2 * t)
 
-    def feed(i):
+    per = chunks // split
+
+    def col(j, back=False):
+        t = split - 1 - j // per if back else j // per
+        return (t + side * (split - 1 - 2 * t)) * per + j % per
+
+    def near(j):
+        return away(j // per) * per + j % per
+
+    def hid(i):
         tokens = tok_s[target(i)]
         gate = lax.dot_general(tokens, wide_s[0], across, preferred_element_type=f32)
         up = lax.dot_general(tokens, wide_s[1], across, preferred_element_type=f32)
-        hid_s[...] = (gate / (1.0 + jnp.exp(-gate)) * up).astype(bf16)
-        for q in range(chunks):
-            ff_s[i, q] = jnp.dot(
-                hid_s[...], wide_s[2, :, q * chunk : (q + 1) * chunk], preferred_element_type=f32
-            ).astype(bf16)
-            tp_copy(i, q).start()
+        hid_s[i] = (gate / (1.0 + jnp.exp(-gate)) * up).astype(bf16)
+
+    def offer(i, js):
+        js = list(js)
+        for at in range(len(js) + 1):
+            if at < len(js):
+                part(i, near(js[at]))
+            if at:
+                lead(i, near(js[at - 1]))
 
     def tp_copy(i, q):
         return remote(
@@ -588,99 +622,170 @@
             {"tp": 1 - core},
         )
 
-    mate = rank + 1 - 2 * lax.rem(rank, 2)
-    ahead = rank + 1 - 2 * side
-
-    def sum_copy(i, q):
-        slot = i + 3 * inner if i < 2 else 2 + inner
-        to = ahead if i < 2 else mate
-        return remote(
-            red_s.at[i, q], rz_s.at[slot, q], ks_sem.at[i, q], kr_sem.at[slot, q],
+    def part(i, q):
+        cols = pl.ds(pl.multiple_of(q * chunk, chunk), chunk)
+        ff_s[i, q] = jnp.dot(
+            hid_s[i], wide_s[2, :, cols], preferred_element_type=f32
+        ).astype(bf16)
+        tp_copy(i, q).start()
+
+    def sum_copy(a, slot, q, to):
+        return remote(
+            red_s.at[a, q], rz_s.at[slot, q], ks_sem.at[a, q], kr_sem.at[slot, q],
             {"sp": to * plane + spot},
-        )
-
-    def sum_landed(slot, q):
-        return remote(
-            red_s.at[0, q], rz_s.at[slot, q], ks_sem.at[0, q], kr_sem.at[slot, q],
-            {"sp": mate * plane + spot},
         )
 
     def pair(i, q):
         tp_copy(i, q).wait()
         return ff_s[i, q, mine, :].astype(f32) + tp_s[i, q].astype(f32)
 
-    def push(i, q):
-        slot = i if i < 2 else 3
-
-        @pl.when(inner == 0)
-        def _():
-            red_s[i, q] = pair(i, q).astype(bf16)
-
-        @pl.when(inner == 1)
-        def _():
-            mixed = pair(i, q)
-            sum_landed(slot, q).wait_recv()
-            red_s[i, q] = (mixed + rz_s[slot, q].astype(f32)).astype(bf16)
-
-        sum_copy(i, q).start()
+    def summed(i, slots, q):
+        mixed = pair(i, q)
+        for slot in slots:
+            sum_copy(0, slot, q, mate).wait_recv()
+            mixed = mixed + rz_s[slot, q].astype(f32)
+        return mixed
+
+    def lead(i, q):
+        red_s[i, q] = summed(i, (), q).astype(bf16)
+        sum_copy(i, i, q, mate).start()
+
+    follow = ((0, 1, 3), (2, 2, 4), (1, 4, 3))
+
+    def trail(a, q):
+        i, slot, out_slot = follow[a]
+        red_s[a, q] = summed(i, (slot,), q).astype(bf16)
+        sum_copy(a, out_slot, q, ahead if a < 2 else mate).start()
 
     def out_copy(q):
-        view = out_ref.at[mine, pl.ds(q * chunk, chunk)]
+        view = out_ref.at[mine, pl.ds(pl.multiple_of(q * chunk, chunk), chunk)]
         return remote(view, view, os_sem.at[q], or_sem.at[q], {"tp": 1 - core})
 
     def out_landed(q):
-        view = out_ref.at[other, pl.ds(q * chunk, chunk)]
+        view = out_ref.at[other, pl.ds(pl.multiple_of(q * chunk, chunk), chunk)]
         return remote(view, view, os_sem.at[q], or_sem.at[q], {"tp": 1 - core})
 
-    def finish(q):
-        cols = slice(q * chunk, (q + 1) * chunk)
-        i = split - 1
-        base = mid_s[mine, cols].astype(f32)
-
-        @pl.when(inner == 0)
-        def _():
-            mixed = pair(i, q)
-            sum_landed(3, q).wait_recv()
-            out_ref[mine, cols] = (base + (mixed + rz_s[3, q].astype(f32))).astype(bf16)
-
-        @pl.when(inner == 1)
-        def _():
-            mixed = pair(i, q)
-            sum_landed(2, q).wait_recv()
-            mixed = mixed + rz_s[2, q].astype(f32)
-            sum_landed(4, q).wait_recv()
-            out_ref[mine, cols] = (base + (mixed + rz_s[4, q].astype(f32))).astype(bf16)
-
+    def finish(role, q):
+        cols = pl.ds(pl.multiple_of(q * chunk, chunk), chunk)
+        total = summed(split - 1, (0, 3) if role else (3,), q)
+        out_ref[mine, cols] = (mid_s[mine, cols].astype(f32) + total).astype(bf16)
         out_copy(q).start()
 
-    feed(0)
-    feed(1)
-    for q in range(chunks):
-        push(0, q)
-    feed(2)
-    for q in range(chunks):
-        push(1, q)
-    feed(3)
-    for q in range(chunks):
-        push(2, q)
-    for q in range(chunks):
-        finish(q)
-
+    first = range(2 * per)
+    second = range(2 * per, chunks)
+
+    tok_start()
+    relay(0, 3)
+    spread(1, 2)
+    relay(1, 1)
+    spread(1, 3)
+    relay(1, 2)
+    spread(2, 1)
+    relay(1, 3)
+    spread(2, 2)
+
+    @pl.when(inner == 0)
+    def outer_plane():
+        for p in range(bits):
+            tok_relay(1, True, p)
+        for c in (0, 1):
+            for k in range(split):
+                settle(c, k)
+        tok_ready(1, True)
+        hid(0)
+        relay(2, 1)
+        settle(2, 0)
+        offer(0, range(per))
+        spread(2, 3)
+        relay(2, 2)
+        settle(2, 1)
+        offer(0, range(per, 2 * per))
+        relay(2, 3)
+        for p in range(bits):
+            tok_relay(2, True, p)
+        tok_ready(2, True)
+        hid(1)
+        offer(1, first)
+        settle(2, 2)
+        offer(1, range(2 * per, 3 * per))
+        settle(2, 3)
+        offer(1, range(3 * per, chunks))
+        for j in second:
+            part(0, near(j))
+        for p in range(bits):
+            tok_relay(3, True, p)
+        tok_ready(3, True)
+        hid(2)
+        offer(2, range(chunks))
+        for j in second:
+            lead(0, near(j))
+        hid(3)
+        for j in range(chunks):
+            part(3, near(j))
+        for j in range(chunks):
+            finish(0, col(j, True))
+
+    @pl.when(inner == 1)
+    def inner_plane():
+        relay(2, 1)
+        for p in range(bits):
+            tok_relay(1, True, p)
+        for c in (0, 1):
+            for k in range(split):
+                settle(c, k)
+        for p in range(bits):
+            tok_relay(1, False, p)
+        spread(2, 3)
+        relay(2, 2)
+        tok_ready(1, True)
+        tok_ready(1, False)
+        hid(0)
+        relay(2, 3)
+        hid(3)
+        for p in range(bits):
+            tok_relay(2, False, p)
+        hid(1)
+        for k in range(split):
+            settle(2, k)
+        for j in range(chunks):
+            part(0, col(j))
+        tok_ready(2, False)
+        for j in range(chunks):
+            part(1, col(j))
+        hid(2)
+        for j in range(chunks):
+            trail(0, col(j))
+        for j in range(chunks):
+            part(2, col(j))
+        for j in range(chunks):
+            part(3, col(j))
+        lag = chunks // 2
+        for j in range(chunks + lag):
+            if j < chunks:
+                trail(1, col(j))
+            if j >= lag:
+                trail(2, col(j - lag, True))
+        for j in range(chunks):
+            finish(1, col(j))
+
+    lax.fori_loop(1, n - me, state_sent, 0)
     for q in range(chunks):
         out_copy(q).wait_send()
         out_landed(q).wait_recv()
-        for i in range(split - 1):
-            sum_copy(i, q).wait_send()
+        for a in range(split - 1):
+            sum_copy(a, a, q, mate).wait_send()
     for way in (0, 1):
         for d in range(1, split):
 
             @pl.when(onward(way, d - 1))
             def _():
-                tok_copy(way, d).wait_send()
+                for p in range(bits):
+                    tok_copy(way, d, p).wait_send()
 
             @pl.when(held(way, d))
             def _():
-                tok_pass(way, d, mine).wait_send()
+                for p in range(bits):
+                    tok_pass(way, d, p, core).wait_send()
 
     for c in range(kinds):
         for k in range(split):
@@ -700,7 +805,7 @@
     kinds = 3
     cut = 512
     pieces = width // cut
-    chunk = width // 2
+    chunk = width // 4
     chunks = width // chunk
     half = rows // 2
     vmem = pl.BlockSpec(memory_space=pltpu.VMEM)
@@ -738,7 +843,7 @@
             buf((rows, width), bf16),
             buf((split, rows, width), bf16),
             buf((kinds, span, width), bf16),
-            buf((rows, span), bf16),
+            buf((split, rows, span), bf16),
             buf((split, chunks, rows, chunk), bf16),
             buf((split, chunks, half, chunk), bf16),
             buf((split - 1, chunks, half, chunk), bf16),
@@ -758,10 +863,10 @@
             dma((kinds, split, 2)),
             dma((pieces,)),
             dma((pieces,)),
-            dma((2, split - 1)),
-            dma((2, split - 1)),
-            dma((2, split - 1)),
-            dma((2, split - 1)),
+            dma((2, split - 1, 2)),
+            dma((2, split - 1, 2)),
+            dma((2, split - 1, 2)),
+            dma((2, split - 1, 2)),
             dma((split, chunks)),
             dma((split, chunks)),
             dma((split - 1, chunks)),
@@ -770,7 +875,7 @@
             dma((chunks,)),
         ],
         compiler_params=pltpu.CompilerParams(
-            collective_id=1, has_side_effects=True, vmem_limit_bytes=60 << 20
+            collective_id=1, has_side_effects=True, vmem_limit_bytes=54 << 20
         ),
         name="layer",
     )(x, bg, extra, taps, dp, wr, wa, ow, res, gain, gw, uw, dw)

time: 146 us -> 128 us (0.88); the launches traced: 144 us -> 128 us
  Pallas kernels: 142 us -> 126 us
    pallas_call x1, Pallas kernels: 142 us -> 126 us  [layer(): pl.pallas_call(functools.partial(layer_kernel, n, split), out_shape=jax.S...]
where the time goes in v2:
time: 128 us
  Pallas kernels  126 us (98%)
  local copies, waits for them, and re-layouts  2.3 us (2%)
    pallas_call x1, Pallas kernels, layer(): pl.pallas_call(functools.partial(layer_kernel, n, split), out_shape=jax.S...  126 us

profile of v2, /device:TPU:0, one launch (start us, length us, event | category | flops | bytes accessed | tf_op | source)
XLA Modules:
  0.0 128.0 jit_solution(2804246394961640509)
XLA Ops:
  0.0 125.7 %layer.1 = bf16[256,2048]{1,0:T(8,128)(2,1)} custom-call(bf16[1024,256]{1,0:T(8,128)(2,1)} %x_ref.1, bf16[1024,256]{1,0:T(8,128)(2,1)} %bg_ref.1, f32[1024,256]{1,0:T(8,128)} %extra_ref.1, bf16[4,1024]{1,0:T(4,128)(2,1)} %bitcast.3, f32[8,128]{1,0:T(8,128)} %bitcast.4, bf16[16,64,64]{2,1,0:T(8,128)(2,1)} %wr_ref.1, bf16[16,64,64]{2,1,0:T(8,128)(2,1)} %wa_ref.1, ...), custom_call_target="tpu_custom_call" | custom-call | tf_op jit(solution)/shard_map/layer/pallas_call | solution.py:816
  125.7 2.3 %copy.15 = bf16[256,2048]{1,0:T(8,128)(2,1)} copy(bf16[256,2048]{1,0:T(8,128)(2,1)} %layer.1) | data formatting | bytes 2097152

commit v3 on v2

--- a/solution.py
+++ b/solution.py
@@ -428,7 +428,6 @@
 
     lax.fori_loop(1, n - me, state_send, 0)
     z_start(1)
-    z_start(2)
     spread(0, 1)
     relay(0, 0)
     spread(2, 0)
@@ -495,6 +494,7 @@
             mix_s[...], ow_s[:, i * cut : (i + 1) * cut], preferred_element_type=f32
         ).astype(bf16)
         swap(i).start()
+    z_start(2)
     relay(0, 2)
     loads[7].wait()
     square = jnp.zeros((row_count, 1), f32)
@@ -676,16 +676,25 @@
 
     tok_start()
     relay(0, 3)
+
+    @pl.when(inner == 0)
+    def _():
+        relay(1, 1)
+
     spread(1, 2)
-    relay(1, 1)
+
+    @pl.when(inner == 1)
+    def _():
+        relay(1, 1)
+
     spread(1, 3)
-    relay(1, 2)
-    spread(2, 1)
-    relay(1, 3)
-    spread(2, 2)
 
     @pl.when(inner == 0)
     def outer_plane():
+        relay(1, 2)
+        relay(1, 3)
+        spread(2, 1)
+        spread(2, 2)
         for p in range(bits):
             tok_relay(1, True, p)
         for c in (0, 1):
@@ -693,13 +702,16 @@
                 settle(c, k)
         tok_ready(1, True)
         hid(0)
+        settle(2, 0)
+        for j in range(per):
+            part(0, near(j))
         relay(2, 1)
-        settle(2, 0)
-        offer(0, range(per))
+        for j in range(per):
+            lead(0, near(j))
         spread(2, 3)
-        relay(2, 2)
         settle(2, 1)
         offer(0, range(per, 2 * per))
+        relay(2, 2)
         relay(2, 3)
         for p in range(bits):
             tok_relay(2, True, p)
@@ -710,14 +722,15 @@
         offer(1, range(2 * per, 3 * per))
         settle(2, 3)
         offer(1, range(3 * per, chunks))
-        for j in second:
+        offer(0, range(2 * per, 3 * per))
+        for j in range(3 * per, chunks):
             part(0, near(j))
         for p in range(bits):
             tok_relay(3, True, p)
         tok_ready(3, True)
         hid(2)
         offer(2, range(chunks))
-        for j in second:
+        for j in range(3 * per, chunks):
             lead(0, near(j))
         hid(3)
         for j in range(chunks):
@@ -727,23 +740,33 @@
 
     @pl.when(inner == 1)
     def inner_plane():
+        relay(1, 2)
+        spread(2, 1)
+        relay(1, 3)
+        spread(2, 2)
+        tok_relay(1, False, 0)
+        for p in range(bits // 2):
+            tok_relay(1, True, p)
         relay(2, 1)
-        for p in range(bits):
+        for p in range(1, bits - 1):
+            tok_relay(1, False, p)
+        for p in range(bits // 2, bits):
             tok_relay(1, True, p)
         for c in (0, 1):
             for k in range(split):
                 settle(c, k)
-        for p in range(bits):
-            tok_relay(1, False, p)
+        tok_relay(1, False, bits - 1)
         spread(2, 3)
         relay(2, 2)
         tok_ready(1, True)
         tok_ready(1, False)
         hid(0)
+        tok_relay(2, False, 0)
         relay(2, 3)
+        for p in range(1, bits - 1):
+            tok_relay(2, False, p)
         hid(3)
-        for p in range(bits):
-            tok_relay(2, False, p)
+        tok_relay(2, False, bits - 1)
         hid(1)
         for k in range(split):
             settle(2, k)
@@ -754,11 +777,11 @@
             part(1, col(j))
         hid(2)
         for j in range(chunks):
-            trail(0, col(j))
-        for j in range(chunks):
             part(2, col(j))
         for j in range(chunks):
             part(3, col(j))
+        for j in range(chunks):
+            trail(0, col(j))
         lag = chunks // 2
         for j in range(chunks + lag):
             if j < chunks:
@@ -815,7 +838,7 @@
     buf = pltpu.VMEM
     return pl.pallas_call(
         functools.partial(layer_kernel, n, split),
-        out_shape=jax.ShapeDtypeStruct((rows, width), bf16),
+        out_shape=pltpu.VMEM((rows, width), bf16),
         in_specs=[hbm, hbm, hbm, vmem, vmem, vmem, vmem, hbm, hbm, vmem, hbm, hbm, hbm],
         out_specs=vmem,
         scratch_shapes=[
@@ -863,10 +886,10 @@
             dma((kinds, split, 2)),
             dma((pieces,)),
             dma((pieces,)),
-            dma((2, split - 1, 2)),
-            dma((2, split - 1, 2)),
-            dma((2, split - 1, 2)),
-            dma((2, split - 1, 2)),
+            dma((2, split - 1, 4)),
+            dma((2, split - 1, 4)),
+            dma((2, split - 1, 4)),
+            dma((2, split - 1, 4)),
             dma((split, chunks)),
             dma((split, chunks)),
             dma((split - 1, chunks)),

time: 128 us -> 124 us (0.969)
  Pallas kernels: 126 us -> 123 us
  local copies, waits for them, and re-layouts: 2.3 us -> 0.97 us
    pallas_call x1, Pallas kernels: 126 us -> 123 us  [layer(): pl.pallas_call(functools.partial(layer_kernel, n, split), out_shape=pltpu...]
    unnamed x1, local copies, waits for them, and re-layouts: 2.3 us -> 0.97 us
where the time goes in v3:
time: 124 us
  Pallas kernels  123 us (99%)
    pallas_call x1, Pallas kernels, layer(): pl.pallas_call(functools.partial(layer_kernel, n, split), out_shape=pltpu...  123 us

profile of v3, /device:TPU:0, one launch (start us, length us, event | category | flops | bytes accessed | tf_op | source)
XLA Modules:
  0.0 123.8 jit_solution(6824651219539240791)
XLA Ops:
  0.0 122.9 %layer.1 = bf16[256,2048]{1,0:T(8,128)(2,1)S(1)} custom-call(bf16[1024,256]{1,0:T(8,128)(2,1)} %x_ref.1, bf16[1024,256]{1,0:T(8,128)(2,1)} %bg_ref.1, f32[1024,256]{1,0:T(8,128)} %extra_ref.1, bf16[4,1024]{1,0:T(4,128)(2,1)} %bitcast.3, f32[8,128]{1,0:T(8,128)} %bitcast.4, bf16[16,64,64]{2,1,0:T(8,128)(2,1)} %wr_ref.1, bf16[16,64,64]{2,1,0:T(8,128)(2,1)} %wa_ref.1, ...), custom_call_target="tpu_custom_call" | custom-call | tf_op jit(solution)/shard_map/layer/pallas_call | solution.py:839
  122.9 1.0 copy.15

commit v4 on v3

--- a/solution.py
+++ b/solution.py
@@ -722,15 +722,14 @@
         offer(1, range(2 * per, 3 * per))
         settle(2, 3)
         offer(1, range(3 * per, chunks))
-        offer(0, range(2 * per, 3 * per))
-        for j in range(3 * per, chunks):
+        for j in second:
             part(0, near(j))
         for p in range(bits):
             tok_relay(3, True, p)
         tok_ready(3, True)
         hid(2)
         offer(2, range(chunks))
-        for j in range(3 * per, chunks):
+        for j in second:
             lead(0, near(j))
         hid(3)
         for j in range(chunks):

time: 124 us -> 123 us (level)
  no operation moved by 1% of the time
where the time goes in v4:
time: 123 us
  Pallas kernels  122 us (99%)
    pallas_call x1, Pallas kernels, layer(): pl.pallas_call(functools.partial(layer_kernel, n, split), out_shape=pltpu...  122 us

profile of v4, /device:TPU:0, one launch (start us, length us, event | category | flops | bytes accessed | tf_op | source)
XLA Modules:
  0.0 123.3 jit_solution(17235772809886844449)
XLA Ops:
  0.0 122.3 %layer.1 = bf16[256,2048]{1,0:T(8,128)(2,1)S(1)} custom-call(bf16[1024,256]{1,0:T(8,128)(2,1)} %x_ref.1, bf16[1024,256]{1,0:T(8,128)(2,1)} %bg_ref.1, f32[1024,256]{1,0:T(8,128)} %extra_ref.1, bf16[4,1024]{1,0:T(4,128)(2,1)} %bitcast.3, f32[8,128]{1,0:T(8,128)} %bitcast.4, bf16[16,64,64]{2,1,0:T(8,128)(2,1)} %wr_ref.1, bf16[16,64,64]{2,1,0:T(8,128)(2,1)} %wa_ref.1, ...), custom_call_target="tpu_custom_call" | custom-call | tf_op jit(solution)/shard_map/layer/pallas_call | solution.py:838
  122.3 1.0 copy.15
